TPU v7x, 512 devices: a whole 4x4x16 slice. The times are simulated.
512 devices in a mesh: sp: 16 (over y, x), tp: 32 (over z, core).
Axes of the slice: x: 4, y: 4, z: 16, core: 2. Of those that a mesh axis runs over, the one named last changes fastest.
Arguments:
- tokens: bfloat16 [8, 49152, 2048], P(None, ('sp', 'tp')), may hold values from -13 to 13
- in_gain: float32 [2048], replicated, may hold values from 0.1 to 1.9
- w_key: bfloat16 [2048, 512], P('tp'), may hold values from -0.125 to 0.125
- w_value: bfloat16 [2048, 512], P('tp'), may hold values from -0.125 to 0.125
- k_gain: float32 [128], replicated, may hold values from 0.1 to 1.9
- new_query: bfloat16 [8, 1024], replicated, may hold values from -6 to 6
- q_gain: float32 [128], replicated, may hold values from 0.1 to 1.9
- stick_bias: float32 [8], replicated, may hold values from -13 to -3
Outputs:
- key_cache: bfloat16 [32, 49152, 128], P('tp', 'sp')
- value_cache: bfloat16 [32, 49152, 128], P('tp', 'sp')
- read_out: float32 [32, 256], P('tp')
All inputs are finite; a program needn't handle non-finite values.
Results may differ from a plain program's by a relative error of at most 0.005.
Values may be sent and summed in bfloat16 or wider, within the bound.
No kernel may reach another device: no remote copies, remote signals or barrier semaphores. Data moves between devices by JAX's collectives and lax.ppermute only.
A program may use at most 64 MiB of HBM per device.

v0:
```python
import jax
import jax.numpy as jnp
from jax import lax
from jax.sharding import PartitionSpec as P

NORM_EPS = 1e-06


def in_one_piece(arrays, axis, dim, along):
    both = jnp.concatenate(arrays, axis=along)
    filled, at, outs = (lax.all_gather(both, axis, axis=dim, tiled=True), 0, [])
    for a in arrays:
        outs.append(lax.slice_in_dim(filled, at, at + a.shape[along], axis=along))
        at += a.shape[along]
    return tuple(outs)


def entering(value, axis, join, neutral):
    count, mine = (lax.axis_size(axis), lax.axis_index(axis))
    pieces = lax.all_gather(value, axis)
    pieces = pieces[::-1]
    mine = count - 1 - mine
    so_far = jnp.full_like(value, 0) + jnp.asarray(neutral, value.dtype)

    def turn(position, so_far):
        longer = join(so_far, pieces[position])
        return jnp.where(position < mine, longer, so_far)

    return lax.fori_loop(0, count - 1, turn, so_far)


def from_everyone(shard, axis):
    length = lax.axis_size(axis)
    return lax.all_to_all(
        jnp.broadcast_to(shard[None], (length, *shard.shape)), axis, 0, 0, tiled=True
    )


def of_everyone(shard, axis):
    everything = from_everyone(shard, axis)
    return jnp.sum(everything, axis=0)


def root_norm(values, scaling):
    inverse = lax.rsqrt(jnp.mean(values * values, axis=-1, keepdims=True) + NORM_EPS)
    return values * inverse * scaling


def add_later(earlier, later_part):
    return earlier + later_part


def shards(tokens, in_gain, w_key, w_value, k_gain, new_query, q_gain, stick_bias):
    seq_count, tok_seq, model_width = tokens.shape
    row_count = seq_count * tok_seq
    head_dim = k_gain.shape[0]
    kv_width = w_key.shape[1]
    kv_heads = kv_width // head_dim
    per_group = stick_bias.shape[0] // kv_heads
    inv_root = head_dim ** (-0.5)
    normed = root_norm(tokens.reshape(row_count, model_width).astype(jnp.float32), in_gain).astype(
        jnp.bfloat16
    )
    pieces = in_one_piece((w_key, w_value), "tp", 0, 1)
    key_raw = jnp.dot(normed, pieces[0], preferred_element_type=jnp.float32)
    value_raw = jnp.dot(normed, pieces[1], preferred_element_type=jnp.float32)
    key_rows = root_norm(key_raw.reshape(seq_count, tok_seq, kv_heads, head_dim), k_gain).astype(
        jnp.bfloat16
    )
    value_rows = value_raw.astype(jnp.bfloat16).reshape(seq_count, tok_seq, kv_heads, head_dim)
    query_rows = root_norm(
        new_query.astype(jnp.float32).reshape(seq_count, kv_heads, per_group, head_dim), q_gain
    ).astype(jnp.bfloat16)
    bias_rows = stick_bias.reshape(kv_heads, per_group)
    key_block = key_rows.transpose(2, 0, 1, 3).reshape(kv_heads * seq_count, tok_seq, head_dim)
    value_block = value_rows.transpose(2, 0, 1, 3).reshape(kv_heads * seq_count, tok_seq, head_dim)
    key_cache, value_cache = (
        lax.all_to_all(key_block, "tp", split_axis=0, concat_axis=1, tiled=True),
        lax.all_to_all(value_block, "tp", split_axis=0, concat_axis=1, tiled=True),
    )
    group_rows = key_cache.shape[0]
    row_start = lax.axis_index("tp") * group_rows
    query_flat = query_rows.transpose(1, 0, 2, 3).reshape(kv_heads * seq_count, per_group, head_dim)
    query_group = lax.dynamic_slice_in_dim(query_flat, row_start, group_rows, 0)
    bias_group = lax.dynamic_slice_in_dim(
        jnp.repeat(bias_rows, seq_count, axis=0), row_start, group_rows, 0
    )
    scores = (
        jnp.einsum("rqe,rpe->rqp", query_group, key_cache, preferred_element_type=jnp.float32)
        * inv_root
        + bias_group[:, :, None]
    )
    log_keep = jax.nn.log_sigmoid(-scores)
    log_total = jnp.sum(log_keep, axis=2)
    log_later = entering(log_total, "sp", add_later, jnp.zeros_like(log_total))
    log_after = log_later[:, :, None] + lax.cumsum(log_keep, axis=2, reverse=True) - log_keep
    weights = jnp.exp(jax.nn.log_sigmoid(scores) + log_after).astype(jnp.bfloat16)
    partial_value = jnp.einsum(
        "rqp,rpe->rqe", weights, value_cache, preferred_element_type=jnp.float32
    )
    read_out = of_everyone(partial_value.reshape(group_rows, per_group * head_dim), "sp")
    return (key_cache, value_cache, read_out)


def solution(mesh):
    return jax.shard_map(
        shards,
        mesh=mesh,
        in_specs=(
            P(None, ("sp", "tp"), None),
            P(),
            P("tp", None),
            P("tp", None),
            P(),
            P(),
            P(),
            P(),
        ),
        out_specs=(P("tp", "sp", None), P("tp", "sp", None), P("tp", None)),
        check_vma=False,
    )
```

profile of v0, /device:TPU:1, one launch (start us, length us, event | category | flops | bytes accessed | tf_op | source)
XLA Modules:
  0.0 228.2 jit_solution(18228065235646988775)
XLA Ops:
  7.2 1.5 pad_maximum_fusion
  8.8 2.6 %multiply_reduce_fusion = f32[8,96]{1,0:T(8,128)S(1)} fusion(bf16[8,96,2048]{2,1,0:T(8,128)(2,1)} %param.10), kind=kLoop, calls=%fused_computation.6 | loop fusion | flops 4717824 | bytes 3148800 | tf_op jit(solution)/shard_map/reduce_sum | solution.py:45
  11.4 78.4 %all-gather.3.cloned.1.call-done = bf16[2048,1024]{1,0:T(8,128)(2,1)} async-done(((bf16[64,1024]{1,0:T(8,128)(2,1)}), bf16[2048,1024]{1,0:T(8,128)(2,1)}) %all-gather.3.cloned.1.call-update) | async-done | bytes 4194320 | tf_op jit(solution)/shard_map/all_gather | solution.py:11
  89.7 3.1 %slice_bitcast_fusion = bf16[512,2048]{0,1:T(8,128)(2,1)} fusion(bf16[2048,1024]{1,0:T(8,128)(2,1)} %all-gather.3.cloned.1.call-done), kind=kLoop, calls=%fused_computation.16 | loop fusion | bytes 4194304 | tf_op jit(solution)/shard_map/dot_general | solution.py:65
  92.8 4.1 %copy.31 = bf16[512,2048]{1,0:T(8,128)(2,1)} copy(bf16[512,2048]{0,1:T(8,128)(2,1)} %slice_bitcast_fusion) | data formatting | bytes 4194304 | tf_op jit(solution)/shard_map/dot_general | solution.py:65
  97.0 3.9 %multiply_reduce_fusion.1 = (f32[8,96,4]{1,2,0:T(4,128)S(1)}, f32[8,96,4,128]{3,1,2,0:T(8,128)S(1)}) fusion(bf16[4,128,2048,1]{2,1,0,3:T(8,128)(2,1)} %bitcast.92, f32[2048]{0:T(1024)S(1)} %copy-done.3, f32[8,96]{1,0:T(8,128)S(1)} %add_rsqrt_fusion.1, bf16[8,96,2048]{2,1,0:T(8,128)(2,1)S(1)} %copy-done), kind=kOutput, calls=%fused_computation.20 | convolution fusion | flops 1617687552 | bytes 6839296 | tf_op jit(solution)/shard_map/dot_general | solution.py:65
  101.4 0.9 copy.32
  102.3 8.2 %all-to-all-start = ((bf16[32,96,128]{2,1,0:T(8,128)(2,1)}), bf16[32,96,128]{2,1,0:T(8,128)(2,1)}, u32[]{:S(2)}, u32[]{:S(2)}) async-start(bf16[32,96,128]{2,1,0:T(8,128)(2,1)} %bitcast.91), calls=%async_computation | async-start | bytes 1572864 | tf_op jit(solution)/shard_map/all_to_all | solution.py:78
  110.9 1.3 dynamic-slice
  113.2 0.8 fusion.1
  114.0 1.4 copy-done.1
  115.4 1.8 fusion.13
  117.4 1.0 copy.33
  118.4 36.7 %all-to-all-done = bf16[32,96,128]{2,1,0:T(8,128)(2,1)} async-done(((bf16[32,96,128]{2,1,0:T(8,128)(2,1)}), bf16[32,96,128]{2,1,0:T(8,128)(2,1)}, u32[]{:S(2)}, u32[]{:S(2)}) %all-to-all-start) | async-done | bytes 786464 | tf_op jit(solution)/shard_map/all_to_all | solution.py:78
  155.2 4.1 %all-to-all-start.1 = ((bf16[32,96,128]{2,1,0:T(8,128)(2,1)}), bf16[32,96,128]{2,1,0:T(8,128)(2,1)S(1)}, u32[]{:S(2)}, u32[]{:S(2)}) async-start(bf16[32,96,128]{2,1,0:T(8,128)(2,1)} %bitcast.11), calls=%async_computation.1 | async-start | bytes 1572864 | tf_op jit(solution)/shard_map/all_to_all | solution.py:79
  159.2 1.4 fusion.2
  161.0 34.8 %all-reduce = f32[32]{0:T(128)S(1)} all-reduce(f32[32]{0:T(128)S(1)} %negate_dynamic-update-slice_fusion), channel_id=2, replica_groups=mesh['sp'=16,'tp'=32] {'sp'}, use_global_device_ids=true, to_apply=%add | all-reduce | flops 32 | bytes 256
  195.9 2.5 %reduce-window.6 = f32[1,2,24,128]{3,2,1,0:T(8,128)S(1)} reduce-window(f32[1,2,24,128]{3,2,1,0:T(8,128)S(1)} %copy.58, f32[]{:T(128)} %constant.49.clone.1), window={size=1x1x1x128 pad=0_0x0_0x0_0x0_127}, to_apply=%region_6.7 | reduce-window | flops 780288 | bytes 49156 | tf_op jit(solution)/shard_map/reduce-window
  199.5 4.5 %all-to-all-done.1 = bf16[32,96,128]{2,1,0:T(8,128)(2,1)S(1)} async-done(((bf16[32,96,128]{2,1,0:T(8,128)(2,1)}), bf16[32,96,128]{2,1,0:T(8,128)(2,1)S(1)}, u32[]{:S(2)}, u32[]{:S(2)}) %all-to-all-start.1) | async-done | bytes 786464 | tf_op jit(solution)/shard_map/all_to_all | solution.py:79
  204.2 0.6 broadcast_in_dim.8
  204.9 6.5 %all-to-all-start.2 = ((f32[16,1,256]{2,1,0:T(1,128)}), f32[16,1,256]{2,1,0:T(1,128)S(1)}, u32[]{:S(2)}, u32[]{:S(2)}) async-start(f32[16,1,256]{2,1,0:T(1,128)} %broadcast_in_dim.8), calls=%async_computation.2 | async-start | bytes 32768 | tf_op jit(solution)/shard_map/all_to_all | solution.py:34
  211.4 6.4 %all-to-all-done.2 = f32[16,1,256]{2,1,0:T(1,128)S(1)} async-done(((f32[16,1,256]{2,1,0:T(1,128)}), f32[16,1,256]{2,1,0:T(1,128)S(1)}, u32[]{:S(2)}, u32[]{:S(2)}) %all-to-all-start.2) | async-done | bytes 16416 | tf_op jit(solution)/shard_map/all_to_all | solution.py:34
  218.4 2.1 copy.68
  220.5 0.9 copy.69
  (58 shorter events, 4.1 us)
Async XLA Ops:
  7.2 82.6 %all-gather.3.cloned.1.call-start = ((), (), s32[]{:S(2)}) async-start(), calls=%async_computation.3 | async-start | bytes 4325376 | tf_op jit(solution)/shard_map/all_gather | solution.py:11
  92.8 4.2 %copy-start = (bf16[8,96,2048]{2,1,0:T(8,128)(2,1)S(1)}, bf16[8,96,2048]{2,1,0:T(8,128)(2,1)}, u32[]{:S(2)}) copy-start(bf16[8,96,2048]{2,1,0:T(8,128)(2,1)} %param.10) | copy-start | bytes 9437188
  92.8 4.2 %copy-start.3 = (f32[2048]{0:T(1024)S(1)}, f32[2048]{0:T(1024)}, u32[]{:S(2)}) copy-start(f32[2048]{0:T(1024)} %param.11) | copy-start | bytes 24580
  97.0 3.9 %copy-start.6 = (f32[128]{0:T(128)S(1)}, f32[128]{0:T(128)}, u32[]{:S(2)}) copy-start(f32[128]{0:T(128)} %param.14) | copy-start | bytes 1540
  100.8 9.7 %copy-start.5 = (f32[8]{0:T(128)S(1)}, f32[8]{0:T(128)}, u32[]{:S(2)}) copy-start(f32[8]{0:T(128)} %param.17) | copy-start | bytes 100
  100.8 12.2 %copy-start.2 = (bf16[8,1024]{1,0:T(8,128)(2,1)S(1)}, bf16[8,1024]{1,0:T(8,128)(2,1)}, u32[]{:S(2)}) copy-start(bf16[8,1024]{1,0:T(8,128)(2,1)} %param.15) | copy-start | bytes 49156
  100.8 12.3 %copy-start.4 = (f32[128]{0:T(128)S(1)}, f32[128]{0:T(128)}, u32[]{:S(2)}) copy-start(f32[128]{0:T(128)} %param.16) | copy-start | bytes 1540
  102.3 52.8 %all-to-all-start = ((bf16[32,96,128]{2,1,0:T(8,128)(2,1)}), bf16[32,96,128]{2,1,0:T(8,128)(2,1)}, u32[]{:S(2)}, u32[]{:S(2)}) async-start(bf16[32,96,128]{2,1,0:T(8,128)(2,1)} %bitcast.91), calls=%async_computation | async-start | bytes 1572864 | tf_op jit(solution)/shard_map/all_to_all | solution.py:78
  113.2 2.2 copy-start.1
  155.2 48.8 %all-to-all-start.1 = ((bf16[32,96,128]{2,1,0:T(8,128)(2,1)}), bf16[32,96,128]{2,1,0:T(8,128)(2,1)S(1)}, u32[]{:S(2)}, u32[]{:S(2)}) async-start(bf16[32,96,128]{2,1,0:T(8,128)(2,1)} %bitcast.11), calls=%async_computation.1 | async-start | bytes 1572864 | tf_op jit(solution)/shard_map/all_to_all | solution.py:79
  204.9 13.0 %all-to-all-start.2 = ((f32[16,1,256]{2,1,0:T(1,128)}), f32[16,1,256]{2,1,0:T(1,128)S(1)}, u32[]{:S(2)}, u32[]{:S(2)}) async-start(f32[16,1,256]{2,1,0:T(1,128)} %broadcast_in_dim.8), calls=%async_computation.2 | async-start | bytes 32768 | tf_op jit(solution)/shard_map/all_to_all | solution.py:34
Sparse Core Ops, SparseCore 0:
  10.7 79.0 all-gather.2
where the time goes:
time: 229 us; the launch traced here: 228 us
  waiting for transfers between devices  126 us (55%)
  blocking collectives  34.8 us (15%)
  starting transfers between devices  18.8 us (8%)
  local copies, waits for them, and re-layouts  16.5 us (7%)
  between operations  14.9 us (7%)
  other arithmetic  9.44 us (4%)
  matrix products  7.38 us (3%)
    all_gather x1, waiting for transfers between devices, in_one_piece(): filled, at, outs = (lax.all_gather(both, axis, axis=dim, tiled=True), 0, [])  78.4 us
    all_to_all x1, waiting for transfers between devices, shards(): lax.all_to_all(key_block, 'tp', split_axis=0, concat_axis=1, tiled=True)  36.7 us
    unnamed x1, blocking collectives  34.8 us
    all_to_all x1, starting transfers between devices, shards(): lax.all_to_all(key_block, 'tp', split_axis=0, concat_axis=1, tiled=True)  8.16 us
    dot_general x2, local copies, waits for them, and re-layouts, shards(): key_raw = jnp.dot(normed, pieces[0], preferred_element_type=jnp.float32)  7.2 us
    all_to_all x1, starting transfers between devices, from_everyone(): lax.all_to_all(jnp.broadcast_to(shard[None], (length, *shard.shape)), axi...  6.53 us
    all_to_all x1, waiting for transfers between devices, from_everyone(): lax.all_to_all(jnp.broadcast_to(shard[None], (length, *shard.shape)), axi...  6.44 us
    unnamed x20, local copies, waits for them, and re-layouts  5.7 us
  transfers between devices with their start and end apart: 4, of which 4 were waited for; matrix products, arithmetic and copies ran while one was open for 6% of the time, Pallas kernels for 0%

commit v1 on v0

v1 whole, which is shorter than its diff:
```python
import functools

import jax
import jax.numpy as jnp
from jax import lax
from jax.experimental import pallas as pl
from jax.experimental.pallas import tpu as pltpu
from jax.sharding import Mesh
from jax.sharding import PartitionSpec as P

NORM_EPS = 1e-06
SP = ("y", "x")
EXTRA = 8
F32 = jnp.float32
BF16 = jnp.bfloat16


def root_norm(values, scaling):
    inverse = lax.rsqrt(jnp.mean(values * values, axis=-1, keepdims=True) + NORM_EPS)
    return values * inverse * scaling


def to_all(piece, axis):
    count = lax.axis_size(axis)
    return lax.all_to_all(
        jnp.broadcast_to(piece[None], (count, *piece.shape)), axis, 0, 0, tiled=True
    )


def gathered_rows(w_key, w_value):
    columns = lax.axis_size(SP)
    mine = lax.axis_index(SP)
    per = columns // 2
    rows = w_key.shape[0] // per
    at = (mine % per) * rows
    piece = jnp.where(
        mine < per,
        lax.dynamic_slice_in_dim(w_key, at, rows, 0),
        lax.dynamic_slice_in_dim(w_value, at, rows, 0),
    )
    along_z = to_all(piece, "z")
    return to_all(along_z, SP)


def high_low(values):
    high = values.astype(BF16)
    return high, (values - high.astype(F32)).astype(BF16)


def project_kernel(
    x_ref, own_ref, other_ref, query_ref, bias_ref, gain_ref, out_ref, wk_ref, wv_ref, sems
):
    core = lax.axis_index("c")
    pieces = own_ref.shape[0] // 2
    rows = own_ref.shape[2]
    seqs = query_ref.shape[0]
    heads = query_ref.shape[1]
    hd = gain_ref.shape[1]
    span = x_ref.shape[0] // seqs
    width = own_ref.shape[3]
    kv_heads = width // hd
    per_group = heads // kv_heads

    def copies(which):
        dst = (wk_ref, wv_ref)[which]
        out = []
        for t, (src, at) in enumerate(((own_ref, core), (other_ref, 1 - core))):
            for r in range(pieces):
                out.append(
                    pltpu.make_async_copy(
                        src.at[which * pieces + r],
                        dst.at[:, at, pl.ds(r * rows, rows), :],
                        sems.at[which, t, r],
                    )
                )
        return out

    key_copies, value_copies = copies(0), copies(1)
    for copy in key_copies + value_copies:
        copy.start()
    x = x_ref[...]
    model = x.shape[1]
    gain = gain_ref[...]
    wide = 2 * hd

    for copy in key_copies:
        copy.wait()
    for h in range(width // wide):
        w = wk_ref[:, :, :, h * wide : (h + 1) * wide].reshape(model, wide)
        raw = jnp.dot(x, w, preferred_element_type=F32)
        for k in range(2):
            g = 2 * h + k
            head = root_norm(raw[:, k * hd : (k + 1) * hd], gain).astype(BF16)
            for i in range(seqs):
                out_ref[g * seqs + i, 0:span, :] = head[i * span : (i + 1) * span]
    for copy in value_copies:
        copy.wait()
    for h in range(width // wide):
        w = wv_ref[:, :, :, h * wide : (h + 1) * wide].reshape(model, wide)
        raw = jnp.dot(x, w, preferred_element_type=F32).astype(BF16)
        for k in range(2):
            g = 2 * h + k
            for i in range(seqs):
                out_ref[g * seqs + i, span : 2 * span, :] = raw[
                    i * span : (i + 1) * span, k * hd : (k + 1) * hd
                ]

    scores = []
    for i in range(seqs):
        total = jnp.zeros((heads, span), F32)
        for g in range(kv_heads):
            total += lax.dot_general(
                query_ref[i, :, g * hd : (g + 1) * hd],
                out_ref[g * seqs + i, 0:span, :],
                (((1,), (1,)), ((), ())),
                preferred_element_type=F32,
            )
        scores.append(total * (hd**-0.5) + bias_ref[...])
    scores = jnp.concatenate(scores, axis=0)
    log_keep = -(jnp.maximum(scores, 0.0) + jnp.log1p(jnp.exp(-jnp.abs(scores))))
    first = lax.broadcasted_iota(jnp.int32, (span, span), 0)
    second = lax.broadcasted_iota(jnp.int32, (span, span), 1)
    later = (first > second).astype(BF16)
    after = jnp.zeros(scores.shape, F32)
    rest = log_keep
    for _ in range(3):
        part = rest.astype(BF16)
        rest = rest - part.astype(F32)
        after += jnp.dot(part, later, preferred_element_type=F32)
    weight_high, weight_low = high_low(jnp.exp(scores + log_keep + after))
    total = jnp.sum(log_keep, axis=1, keepdims=True)
    total_high, total_low = high_low(total)
    put = lax.broadcasted_iota(jnp.int32, (EXTRA, 4 * heads), 0)
    take = lax.broadcasted_iota(jnp.int32, (EXTRA, 4 * heads), 1)
    for i in range(seqs):
        at = slice(i * heads, (i + 1) * heads)
        for g in range(kv_heads):
            values = out_ref[g * seqs + i, span : 2 * span, :]
            read = jnp.dot(weight_high[at], values, preferred_element_type=F32) + jnp.dot(
                weight_low[at], values, preferred_element_type=F32
            )
            read_high, read_low = high_low(read)
            stacked = jnp.concatenate(
                [
                    read_high.astype(F32),
                    read_low.astype(F32),
                    jnp.broadcast_to(total_high[at].astype(F32), read.shape),
                    jnp.broadcast_to(total_low[at].astype(F32), read.shape),
                ],
                axis=0,
            ).astype(BF16)
            pick = (
                take == (put // per_group) * heads + g * per_group + put % per_group
            ).astype(BF16)
            out_ref[g * seqs + i, 2 * span :, :] = jnp.dot(
                pick, stacked, preferred_element_type=F32
            ).astype(BF16)


def project(x, own, other, query, bias, gain):
    seqs, heads, width = query.shape
    hd = gain.shape[1]
    span = x.shape[0] // seqs
    blocks = (width // hd) * seqs
    pieces, zs, rows, _ = own.shape
    half = pieces // 2
    scratch = pltpu.VMEM((zs, 2, half * rows, width), BF16)
    vmem = pl.BlockSpec(memory_space=pltpu.VMEM)
    hbm = pl.BlockSpec(memory_space=pl.ANY)
    return pl.pallas_call(
        project_kernel,
        out_shape=jax.ShapeDtypeStruct((blocks, 2 * span + EXTRA, hd), BF16),
        in_specs=[vmem, hbm, hbm, vmem, vmem, vmem],
        out_specs=vmem,
        scratch_shapes=[scratch, scratch, pltpu.SemaphoreType.DMA((2, 2, half))],
        compiler_params=pltpu.CompilerParams(vmem_limit_bytes=48 * 1024 * 1024),
        name="project",
    )(x, own, other, query, bias, gain)


def join_first_kernel(rows_ref, out_ref):
    count = rows_ref.shape[0]
    shape = (2, rows_ref.shape[2])
    read, log_later = jnp.zeros(shape, F32), jnp.zeros(shape, F32)
    for n in reversed(range(count)):
        rows = rows_ref[n].astype(F32)
        read += jnp.exp(log_later) * (rows[0:2] + rows[2:4])
        log_later += rows[4:6] + rows[6:8]
    out_ref[0:2] = read
    out_ref[2:4] = log_later


def join_last_kernel(rows_ref, out_ref):
    count = rows_ref.shape[0]
    shape = (2, rows_ref.shape[2])
    read, log_later = jnp.zeros(shape, F32), jnp.zeros(shape, F32)
    for n in reversed(range(count)):
        read += jnp.exp(log_later) * rows_ref[n, 0:2]
        log_later += rows_ref[n, 2:4]
    out_ref[...] = read


def join_first(received):
    count, rows, hd = received.shape
    return pl.pallas_call(
        join_first_kernel,
        grid=(1,),
        out_shape=jax.ShapeDtypeStruct((4, hd), F32),
        in_specs=[pl.BlockSpec((count, EXTRA, hd), lambda i: (0, rows // EXTRA - 1, 0))],
        out_specs=pl.BlockSpec((4, hd), lambda i: (0, 0)),
        name="join_first",
    )(received)


def join_last(pieces):
    return pl.pallas_call(
        join_last_kernel,
        out_shape=jax.ShapeDtypeStruct((2, pieces.shape[2]), F32),
        name="join_last",
    )(pieces)


def shards(tokens, in_gain, w_key, w_value, k_gain, new_query, q_gain, stick_bias):
    seq_count, tok_seq, model_width = tokens.shape
    head_dim = k_gain.shape[0]
    heads = stick_bias.shape[0]
    kv_heads = w_key.shape[1] // head_dim
    per_group = heads // kv_heads
    seqs = seq_count // 2
    core = lax.axis_index("c")

    own = gathered_rows(w_key, w_value)
    other = lax.ppermute(own, "c", [(0, 1), (1, 0)])

    paired = tokens.reshape(seqs, 2, tok_seq, model_width)
    kept = lax.dynamic_index_in_dim(paired, core, 1, False)
    sent = lax.dynamic_index_in_dim(paired, 1 - core, 1, False)
    came = lax.ppermute(sent, "c", [(0, 1), (1, 0)])
    low = jnp.where(core == 0, kept, came)
    high = jnp.where(core == 0, came, kept)
    span_tokens = jnp.stack([low, high], axis=1).reshape(seqs * 2 * tok_seq, model_width)
    normed = root_norm(span_tokens.astype(F32), in_gain).astype(BF16)

    query = root_norm(
        new_query.astype(F32).reshape(seqs, 2, heads, head_dim)[:, 0], q_gain
    )
    query_odd = root_norm(
        new_query.astype(F32).reshape(seqs, 2, heads, head_dim)[:, 1], q_gain
    )
    query = jnp.where(core == 0, query, query_odd).astype(BF16)
    of_group = jnp.arange(heads)[:, None] // per_group == jnp.arange(kv_heads)[None, :]
    query = jnp.where(of_group[None, :, :, None], query[:, :, None, :], 0).reshape(
        seqs, heads, kv_heads * head_dim
    )

    out = project(
        normed, own, other, query, stick_bias.reshape(heads, 1), k_gain.reshape(1, head_dim)
    )
    received = lax.all_to_all(out, "z", 0, 0, tiled=True)
    span = 2 * tok_seq
    joined = join_first(received)
    everything = to_all(joined, SP)
    read = join_last(everything)
    positions = received.shape[0] * span
    key_cache = received[:, :span].reshape(1, positions, head_dim)
    value_cache = received[:, span : 2 * span].reshape(1, positions, head_dim)
    return (key_cache, value_cache, read.reshape(1, per_group * head_dim))


def solution(mesh):
    grid = Mesh(mesh.devices.reshape(4, 4, 16, 2), ("y", "x", "z", "c"))
    tp = ("z", "c")
    return jax.shard_map(
        shards,
        mesh=grid,
        in_specs=(
            P(None, ("y", "x", "z", "c"), None),
            P(),
            P(tp, None),
            P(tp, None),
            P(),
            P(),
            P(),
            P(),
        ),
        out_specs=(P(tp, SP, None), P(tp, SP, None), P(tp, None)),
        check_vma=False,
    )
```

time: 229 us -> 190 us (0.83)
  waiting for transfers between devices: 126 us -> 19.7 us
  blocking collectives: 34.8 us -> 113 us
  between operations: 14.9 us -> 0.83 us
  Pallas kernels: 0 us -> 13.3 us
  matrix products: 7.38 us -> 0 us
  local copies, waits for them, and re-layouts: 16.5 us -> 10.2 us
  starting transfers between devices: 18.8 us -> 24.8 us
    all_to_all x0 -> x2, blocking collectives: none -> 113 us  [the longest x1 85.1 us: shards(): received = lax.all_to_all(out, 'z', 0, 0, tiled=True)]
    all_gather x1 -> x0, waiting for transfers between devices: 78.4 us -> none  [in_one_piece(): filled, at, outs = (lax.all_gather(both, axis, axis=dim, tiled=True), 0, [])]
    unnamed x1 -> x0, blocking collectives: 34.8 us -> none
    all_to_all x3 -> x2, waiting for transfers between devices: 47.7 us -> 19.7 us  [to_all(): lax.all_to_all(jnp.broadcast_to(piece[None], (count, *piece.shape)), axis...]
    ppermute x0 -> x2, starting transfers between devices: none -> 14.5 us  [the longest x1 8.53 us: shards(): other = lax.ppermute(own, 'c', [(0, 1), (1, 0)])]
    pallas_call x0 -> x3, Pallas kernels: none -> 13.3 us  [the longest x1 10.5 us: project(): pl.pallas_call(project_kernel, out_shape=jax.ShapeDtypeStruct((blocks, 2...]
    all_to_all x3 -> x2, starting transfers between devices: 18.8 us -> 10.4 us  [to_all(): lax.all_to_all(jnp.broadcast_to(piece[None], (count, *piece.shape)), axis...]
    dot_general x4 -> x0, matrix products: 7.38 us -> none  [the longest x1 3.85 us: shards(): key_raw = jnp.dot(normed, pieces[0], preferred_element_type=jnp.float32)]
  transfers between devices with their start and end apart: 4 -> 4, of which waited for: 4 -> 2; matrix products, arithmetic and copies ran while one was open for 6% -> 7% of each run, Pallas kernels for 0% -> 0%
where the time goes in v1:
time: 190 us
  blocking collectives  113 us (59%)
  starting transfers between devices  24.8 us (13%)
  waiting for transfers between devices  19.7 us (10%)
  Pallas kernels  13.3 us (7%)
  local copies, waits for them, and re-layouts  10.2 us (5%)
  other arithmetic  8.26 us (4%)
    all_to_all x1, blocking collectives, shards(): received = lax.all_to_all(out, 'z', 0, 0, tiled=True)  85.1 us
    all_to_all x1, blocking collectives, to_all(): lax.all_to_all(jnp.broadcast_to(piece[None], (count, *piece.shape)), axis...  27.5 us
    all_to_all x2, waiting for transfers between devices, to_all(): lax.all_to_all(jnp.broadcast_to(piece[None], (count, *piece.shape)), axis...  19.7 us
    pallas_call x1, Pallas kernels, project(): pl.pallas_call(project_kernel, out_shape=jax.ShapeDtypeStruct((blocks, 2...  10.5 us
    all_to_all x2, starting transfers between devices, to_all(): lax.all_to_all(jnp.broadcast_to(piece[None], (count, *piece.shape)), axis...  10.4 us
    ppermute x1, starting transfers between devices, shards(): other = lax.ppermute(own, 'c', [(0, 1), (1, 0)])  8.53 us
    ppermute x1, starting transfers between devices, shards(): came = lax.ppermute(sent, 'c', [(0, 1), (1, 0)])  5.94 us
    convert_element_type x2, other arithmetic, shards(): normed = root_norm(span_tokens.astype(F32), in_gain).astype(BF16)  4.54 us
  transfers between devices with their start and end apart: 4, of which 2 were waited for; matrix products, arithmetic and copies ran while one was open for 7% of the time, Pallas kernels for 0%

profile of v1, /device:TPU:1, one launch (start us, length us, event | category | flops | bytes accessed | tf_op | source)
XLA Modules:
  0.0 189.7 jit_solution(1506460091340135612)
XLA Ops:
  0.7 0.7 dynamic-slice_select_fusion
  1.4 27.5 %all_to_all.20 = bf16[16,8,512]{2,1,0:T(8,128)(2,1)S(1)} all-to-all(bf16[16,8,512]{2,1,0:T(8,128)(2,1)S(1)} %broadcast_in_dim.32), channel_id=1, replica_groups=mesh['y'=4,'x'=4,'z'=16,'c'=2] {'z'}, dimensions={0} | all-to-all | bytes 262144 | tf_op jit(solution)/shard_map/all_to_all | solution.py:25
  28.9 1.5 broadcast_in_dim.33
  30.5 6.9 %all-to-all-start.1 = ((bf16[16,16,8,512]{3,2,1,0:T(8,128)(2,1)}), bf16[16,16,8,512]{3,2,1,0:T(8,128)(2,1)S(1)}, u32[]{:S(2)}, u32[]{:S(2)}) async-start(bf16[16,16,8,512]{3,2,1,0:T(8,128)(2,1)} %broadcast_in_dim.33), calls=%async_computation.1 | async-start | bytes 4194304 | tf_op jit(solution)/shard_map/all_to_all | solution.py:25
  37.3 2.7 %dynamic-slice_bitcast_fusion = bf16[4,96,2048]{2,1,0:T(8,128)(2,1)} fusion(bf16[4,2,96,2048]{3,2,1,0:T(8,128)(2,1)} %bitcast.50, s32[]{:T(128)S(6)} %select_n.67), kind=kLoop, calls=%fused_computation.9 | loop fusion | bytes 3145732 | tf_op jit(solution)/shard_map/jit(dynamic_index_in_dim)/squeeze | solution.py:237
  40.1 5.9 %collective-permute-start = (bf16[4,96,2048]{2,1,0:T(8,128)(2,1)}, bf16[4,96,2048]{2,1,0:T(8,128)(2,1)}, u32[]{:S(2)}, u32[]{:S(2)}) collective-permute-start(bf16[4,96,2048]{2,1,0:T(8,128)(2,1)} %dynamic-slice_bitcast_fusion), channel_id=1, source_target_pairs={{0,1},{1,0},{2,3},{3,2},{4,5},{5,4},{6,7},{7,6},{8,9},{9,8},{10,11... | collective-permute-start | bytes 4718600 | tf_op jit(solution)/shard_map/ppermute | solution.py:238
  46.1 0.1 multiply_reduce_fusion.2
  46.4 15.9 %all-to-all-done.1.own_ref = bf16[16,16,8,512]{3,2,1,0:T(8,128)(2,1)S(1)} async-done(((bf16[16,16,8,512]{3,2,1,0:T(8,128)(2,1)}), bf16[16,16,8,512]{3,2,1,0:T(8,128)(2,1)S(1)}, u32[]{:S(2)}, u32[]{:S(2)}) %all-to-all-start.1) | async-done | bytes 2097184 | tf_op jit(solution)/shard_map/all_to_all | solution.py:25
  62.3 8.5 %collective-permute-start.1 = (bf16[16,16,8,512]{3,2,1,0:T(8,128)(2,1)S(1)}, bf16[16,16,8,512]{3,2,1,0:T(8,128)(2,1)}, u32[]{:S(2)}, u32[]{:S(2)}) collective-permute-start(bf16[16,16,8,512]{3,2,1,0:T(8,128)(2,1)S(1)} %all-to-all-done.1.own_ref), channel_id=1, source_target_pairs={{0,1},{1,0},{2,3},{3,2},{4,5},{5,4},{6,7},{7,6},{8,9},{9,8},{10,11... | collective-permute-start | bytes 6291464 | tf_op jit(solution)/shard_map/ppermute | solution.py:233
  70.9 0.1 copy.13.bias_ref
  70.9 2.1 %fusion.2 = (bf16[4,1,96,2048]{3,2,1,0:T(8,128)(2,1)S(1)}, bf16[4,1,96,2048]{3,2,1,0:T(8,128)(2,1)S(1)}) fusion(bf16[4,96,2048]{2,1,0:T(8,128)(2,1)} %collective-permute-done, pred[]{:T(512)S(6)} %eq.24, bf16[4,2,96,2048]{3,2,1,0:T(8,128)(2,1)} %bitcast.51, s32[]{:T(128)S(6)} %select_n.66), kind=kLoop, calls=%fused_computation.7 | loop fusion | flops 1572864 | bytes 6291461 | tf_op jit(solution)/shard_map/stack | solution.py:241
  73.0 1.1 copy-done.1
  74.2 0.7 multiply_reduce_fusion
  75.0 2.3 %maximum_convert_fusion = f32[4,2,96,2048]{3,2,1,0:T(8,128)S(1)} fusion(bf16[4,1,96,2048]{3,2,1,0:T(8,128)(2,1)} %copy-done.2, bf16[4,1,96,2048]{3,2,1,0:T(8,128)(2,1)} %copy-done.1), kind=kLoop, calls=%fused_computation.4 | loop fusion | flops 3145728 | bytes 9437184 | tf_op jit(solution)/shard_map/convert_element_type | solution.py:242
  77.3 2.2 %fusion.1.x_ref = bf16[768,2048]{1,0:T(8,128)(2,1)} fusion(f32[4,2,96,2048]{3,2,1,0:T(8,128)S(1)} %maximum_convert_fusion, f32[2048]{0:T(1024)S(1)} %copy-done.5, f32[768]{0:T(1024)S(1)} %rsqrt.28), kind=kLoop, calls=%fused_computation.2 | loop fusion | flops 4718592 | bytes 9448448 | tf_op jit(solution)/shard_map/convert_element_type | solution.py:242
  79.5 10.5 %project.1 = bf16[16,392,128]{2,1,0:T(8,128)(2,1)S(1)} custom-call(bf16[768,2048]{1,0:T(8,128)(2,1)} %fusion.1.x_ref, bf16[16,16,8,512]{3,2,1,0:T(8,128)(2,1)S(1)} %all-to-all-done.1.own_ref, bf16[16,16,8,512]{3,2,1,0:T(8,128)(2,1)} %collective-permute-done.1.other_ref, bf16[4,8,512]{2,1,0:T(8,128)(2,1)S(1)} %bitcast_select_fusion.2.query_ref, ...), custom_call_target="tpu_custom_call" | custom-call | tf_op jit(solution)/shard_map/project/pallas_call | solution.py:170
  90.1 85.1 %all_to_all.21.rows_ref = bf16[16,392,128]{2,1,0:T(8,128)(2,1)} all-to-all(bf16[16,392,128]{2,1,0:T(8,128)(2,1)S(1)} %project.1), channel_id=1, replica_groups=mesh['y'=4,'x'=4,'z'=16,'c'=2] {'z'}, dimensions={0} | all-to-all | bytes 3211264 | tf_op jit(solution)/shard_map/all_to_all | solution.py:259
  175.2 1.4 join_first.1
  176.5 1.3 broadcast_in_dim.62
  177.8 3.5 %all-to-all-start.3 = ((f32[16,4,128]{2,1,0:T(4,128)}), f32[16,4,128]{2,1,0:T(4,128)S(1)}, u32[]{:S(2)}, u32[]{:S(2)}) async-start(f32[16,4,128]{2,1,0:T(4,128)} %broadcast_in_dim.62), calls=%async_computation.3 | async-start | bytes 65536 | tf_op jit(solution)/shard_map/all_to_all | solution.py:25
  181.3 2.6 %fusion.4 = (bf16[16,192,128]{2,1,0:T(8,128)(2,1)}, bf16[16,192,128]{2,1,0:T(8,128)(2,1)}) fusion(bf16[16,392,128]{2,1,0:T(8,128)(2,1)} %all_to_all.21.rows_ref), kind=kLoop, calls=%fused_computation.27 | loop fusion | bytes 3145728 | tf_op jit(solution)/shard_map/slice | solution.py:266
  183.9 3.8 %all-to-all-done.3.rows_ref = f32[16,4,128]{2,1,0:T(4,128)S(1)} async-done(((f32[16,4,128]{2,1,0:T(4,128)}), f32[16,4,128]{2,1,0:T(4,128)S(1)}, u32[]{:S(2)}, u32[]{:S(2)}) %all-to-all-start.3) | async-done | bytes 32800 | tf_op jit(solution)/shard_map/all_to_all | solution.py:25
  187.7 0.6 copy-done.3
  188.3 1.3 join_last.1
  (27 shorter events, 0.3 us)
Async XLA Ops:
  30.4 15.6 %copy-start.4 = (bf16[8,1024]{1,0:T(8,128)(2,1)S(1)}, bf16[8,1024]{1,0:T(8,128)(2,1)}, u32[]{:S(2)}) copy-start(bf16[8,1024]{1,0:T(8,128)(2,1)} %param.13) | copy-start | bytes 49156
  30.4 15.8 %copy-start.6 = (f32[128]{0:T(128)S(1)}, f32[128]{0:T(128)}, u32[]{:S(2)}) copy-start(f32[128]{0:T(128)} %param.14) | copy-start | bytes 1540
  30.4 40.4 %copy-start.7 = (f32[8]{0:T(128)S(1)}, f32[8]{0:T(128)}, u32[]{:S(2)}) copy-start(f32[8]{0:T(128)} %param.15) | copy-start | bytes 100
  30.5 31.8 %all-to-all-start.1 = ((bf16[16,16,8,512]{3,2,1,0:T(8,128)(2,1)}), bf16[16,16,8,512]{3,2,1,0:T(8,128)(2,1)S(1)}, u32[]{:S(2)}, u32[]{:S(2)}) async-start(bf16[16,16,8,512]{3,2,1,0:T(8,128)(2,1)} %broadcast_in_dim.33), calls=%async_computation.1 | async-start | bytes 4194304 | tf_op jit(solution)/shard_map/all_to_all | solution.py:25
  40.1 30.8 %collective-permute-start = (bf16[4,96,2048]{2,1,0:T(8,128)(2,1)}, bf16[4,96,2048]{2,1,0:T(8,128)(2,1)}, u32[]{:S(2)}, u32[]{:S(2)}) collective-permute-start(bf16[4,96,2048]{2,1,0:T(8,128)(2,1)} %dynamic-slice_bitcast_fusion), channel_id=1, source_target_pairs={{0,1},{1,0},{2,3},{3,2},{4,5},{5,4},{6,7},{7,6},{8,9},{9,8},{10,11... | collective-permute-start | bytes 4718600 | tf_op jit(solution)/shard_map/ppermute | solution.py:238
  62.3 17.2 %collective-permute-start.1 = (bf16[16,16,8,512]{3,2,1,0:T(8,128)(2,1)S(1)}, bf16[16,16,8,512]{3,2,1,0:T(8,128)(2,1)}, u32[]{:S(2)}, u32[]{:S(2)}) collective-permute-start(bf16[16,16,8,512]{3,2,1,0:T(8,128)(2,1)S(1)} %all-to-all-done.1.own_ref), channel_id=1, source_target_pairs={{0,1},{1,0},{2,3},{3,2},{4,5},{5,4},{6,7},{7,6},{8,9},{9,8},{10,11... | collective-permute-start | bytes 6291464 | tf_op jit(solution)/shard_map/ppermute | solution.py:233
  73.0 1.1 copy-start.1
  73.0 1.8 copy-start.2
  75.0 2.3 %copy-start.5 = (f32[2048]{0:T(1024)S(1)}, f32[2048]{0:T(1024)}, u32[]{:S(2)}) copy-start(f32[2048]{0:T(1024)} %param.9) | copy-start | bytes 24580
  77.3 2.3 %copy-start = (f32[128]{0:T(128)S(1)}, f32[128]{0:T(128)}, u32[]{:S(2)}) copy-start(f32[128]{0:T(128)} %param.12) | copy-start | bytes 1540
  177.8 9.9 %all-to-all-start.3 = ((f32[16,4,128]{2,1,0:T(4,128)}), f32[16,4,128]{2,1,0:T(4,128)S(1)}, u32[]{:S(2)}, u32[]{:S(2)}) async-start(f32[16,4,128]{2,1,0:T(4,128)} %broadcast_in_dim.62), calls=%async_computation.3 | async-start | bytes 65536 | tf_op jit(solution)/shard_map/all_to_all | solution.py:25
  187.7 0.6 copy-start.3

commit v2 on v1

v2 whole, which is shorter than its diff:
```python
import jax
import jax.numpy as jnp
from jax import lax
from jax.experimental import pallas as pl
from jax.experimental.pallas import tpu as pltpu
from jax.sharding import Mesh
from jax.sharding import PartitionSpec as P

NORM_EPS = 1e-06
SP = ("y", "x")
EXTRA = 8
F32 = jnp.float32
BF16 = jnp.bfloat16


def root_norm(values, scaling):
    inverse = lax.rsqrt(jnp.mean(values * values, axis=-1, keepdims=True) + NORM_EPS)
    return values * inverse * scaling


def to_all(piece, axis):
    count = lax.axis_size(axis)
    return lax.all_to_all(
        jnp.broadcast_to(piece[None], (count, *piece.shape)), axis, 0, 0, tiled=True
    )


def along_z(w_key, w_value):
    columns = lax.axis_size(SP)
    mine = lax.axis_index(SP)
    per = columns // 2
    rows = w_key.shape[0] // per
    at = (mine % per) * rows
    piece = jnp.where(
        mine < per,
        lax.dynamic_slice_in_dim(w_key, at, rows, 0),
        lax.dynamic_slice_in_dim(w_value, at, rows, 0),
    )
    return to_all(piece, "z")


def norm_kernel(tokens_ref, gain_ref, kept_ref, sent_ref):
    core = lax.axis_index("c")
    gain = gain_ref[...]
    kept_ref[0] = root_norm(tokens_ref[core].astype(F32), gain).astype(BF16)
    sent_ref[0] = root_norm(tokens_ref[1 - core].astype(F32), gain).astype(BF16)


def norm_halves(tokens, in_gain):
    seq_count, length, model = tokens.shape
    half = jax.ShapeDtypeStruct((seq_count // 2, length, model), BF16)
    block = pl.BlockSpec((1, length, model), lambda i: (i, 0, 0))
    return pl.pallas_call(
        norm_kernel,
        grid=(seq_count // 2,),
        out_shape=(half, half),
        in_specs=[
            pl.BlockSpec((2, length, model), lambda i: (i, 0, 0)),
            pl.BlockSpec((1, model), lambda i: (0, 0)),
        ],
        out_specs=(block, block),
        compiler_params=vmem(16),
        name="norm_halves",
    )(tokens, in_gain.reshape(1, model))


def spread_kernel(piece_ref, out_ref):
    piece = piece_ref[...]
    for n in range(out_ref.shape[0]):
        out_ref[n] = piece


def spread(piece, count):
    return pl.pallas_call(
        spread_kernel,
        out_shape=pltpu.VMEM((count, *piece.shape), piece.dtype),
        compiler_params=vmem(8),
        name="spread",
    )(*on_chip(piece))


def vmem(mib):
    return pltpu.CompilerParams(vmem_limit_bytes=mib * 1024 * 1024)


def on_chip(*arrays):
    return tuple(pltpu.with_memory_space_constraint(a, pltpu.VMEM) for a in arrays)


def high_low(values):
    high = values.astype(BF16)
    return high, (values - high.astype(F32)).astype(BF16)


def arrange_kernel(kept_ref, came_ref, query_ref, gain_ref, x_ref, grouped_ref):
    core = lax.axis_index("c")
    seqs, length, model = kept_ref.shape
    hd = gain_ref.shape[1]
    heads = query_ref.shape[1] // hd
    kv_heads = grouped_ref.shape[2] // hd
    zs = lax.axis_size("z")
    held = model // zs // 2
    rows = hd // zs
    pieces = held // rows
    wide = 2 * hd
    kept = kept_ref[...].reshape(seqs * length, model)
    came = came_ref[...].reshape(seqs * length, model)
    source = lax.broadcasted_iota(jnp.int32, (model, wide), 0)
    column = lax.broadcasted_iota(jnp.int32, (model, wide), 1)
    inside = column % hd
    target = (inside // rows) * (2 * held) + (column // hd) * rows + inside % rows
    offset = source - target
    for half in range(2):
        for r in range(0, pieces, 2):
            pick = (offset == half * held + r * rows).astype(BF16)
            at = slice(r * hd, r * hd + wide)
            x_ref[half, core, :, at] = jnp.dot(kept, pick, preferred_element_type=F32).astype(BF16)
            x_ref[half, 1 - core, :, at] = jnp.dot(
                came, pick, preferred_element_type=F32
            ).astype(BF16)

    query = query_ref[...].astype(F32)
    row = lax.broadcasted_iota(jnp.int32, (heads, hd), 0)
    per_group = heads // kv_heads
    for i in range(seqs):
        mine = jnp.where(core == 0, query[2 * i : 2 * i + 1], query[2 * i + 1 : 2 * i + 2])
        for g in range(kv_heads):
            block = jnp.zeros((heads, hd), F32)
            for j in range(g * per_group, (g + 1) * per_group):
                head = root_norm(mine[:, j * hd : (j + 1) * hd], gain_ref[...])
                block = jnp.where(row == j, head, block)
            grouped_ref[i, :, g * hd : (g + 1) * hd] = block.astype(BF16)


def arrange(kept, came, new_query, q_gain, kv_heads):
    seqs, length, model = kept.shape
    hd = q_gain.shape[0]
    heads = new_query.shape[1] // hd
    return pl.pallas_call(
        arrange_kernel,
        out_shape=(
            pltpu.VMEM((2, 2, seqs * length, model // 2), BF16),
            pltpu.VMEM((seqs, heads, kv_heads * hd), BF16),
        ),
        compiler_params=vmem(32),
        name="arrange",
    )(kept, came, new_query, q_gain.reshape(1, hd))


def partial_kernel(x_ref, rows_ref, out_ref):
    core = lax.axis_index("c")
    x = x_ref[core]
    for which in range(rows_ref.shape[0]):
        out_ref[which] = jnp.dot(x, rows_ref[which], preferred_element_type=F32)


def partial_product(x, own):
    return pl.pallas_call(
        partial_kernel,
        out_shape=pltpu.VMEM((2, x.shape[1], own.shape[2]), F32),
        compiler_params=vmem(16),
        name="partial",
    )(*on_chip(x, own))


def finish_kernel(x_ref, rows_ref, begun_ref, query_ref, bias_ref, gain_ref, key_ref, value_ref):
    core = lax.axis_index("c")
    seqs, heads, width = query_ref.shape
    hd = gain_ref.shape[1]
    length = x_ref.shape[1] // (2 * seqs)
    span = 2 * length
    kv_heads = width // hd
    per_group = heads // kv_heads
    wide = 2 * hd
    x = x_ref[1 - core]
    gain = gain_ref[...]

    def place(ref, g, head):
        for n in range(2 * seqs):
            h, i = divmod(n, seqs)
            ref[g * seqs + i, h * length : (h + 1) * length, :] = head[n * length : (n + 1) * length]

    for start in range(0, width, wide):
        at = slice(start, start + wide)
        raw = begun_ref[0, :, at] + jnp.dot(x, rows_ref[0, :, at], preferred_element_type=F32)
        for k in range(2):
            head = root_norm(raw[:, k * hd : (k + 1) * hd], gain).astype(BF16)
            place(key_ref, start // hd + k, head)

    row = lax.broadcasted_iota(jnp.int32, (heads, 1), 0)
    bias = jnp.zeros((heads, 1), F32)
    for j in range(heads):
        bias = jnp.where(row == j, bias_ref[j], bias)
    scores = []
    for i in range(seqs):
        total = jnp.zeros((heads, span), F32)
        for g in range(kv_heads):
            total += lax.dot_general(
                query_ref[i, :, g * hd : (g + 1) * hd],
                key_ref[g * seqs + i, 0:span, :],
                (((1,), (1,)), ((), ())),
                preferred_element_type=F32,
            )
        scores.append(total * (hd**-0.5) + bias)
    scores = jnp.concatenate(scores, axis=0)
    log_keep = -(jnp.maximum(scores, 0.0) + jnp.log1p(jnp.exp(-jnp.abs(scores))))
    first = lax.broadcasted_iota(jnp.int32, (span, span), 0)
    second = lax.broadcasted_iota(jnp.int32, (span, span), 1)
    later = (first > second).astype(BF16)
    after = jnp.zeros(scores.shape, F32)
    rest = log_keep
    for _ in range(3):
        part = rest.astype(BF16)
        rest = rest - part.astype(F32)
        after += jnp.dot(part, later, preferred_element_type=F32)
    weight_high, weight_low = high_low(jnp.exp(scores + log_keep + after))
    total_high, total_low = high_low(jnp.sum(log_keep, axis=1, keepdims=True))

    for start in range(0, width, wide):
        at = slice(start, start + wide)
        raw = begun_ref[1, :, at] + jnp.dot(x, rows_ref[1, :, at], preferred_element_type=F32)
        for k in range(2):
            place(value_ref, start // hd + k, raw[:, k * hd : (k + 1) * hd].astype(BF16))

    put = lax.broadcasted_iota(jnp.int32, (EXTRA, 4 * heads), 0)
    take = lax.broadcasted_iota(jnp.int32, (EXTRA, 4 * heads), 1)
    for i in range(seqs):
        at = slice(i * heads, (i + 1) * heads)
        for g in range(kv_heads):
            values = value_ref[g * seqs + i]
            read = jnp.dot(weight_high[at], values, preferred_element_type=F32) + jnp.dot(
                weight_low[at], values, preferred_element_type=F32
            )
            read_high, read_low = high_low(read)
            stacked = jnp.concatenate(
                [
                    read_high.astype(F32),
                    read_low.astype(F32),
                    jnp.broadcast_to(total_high[at].astype(F32), read.shape),
                    jnp.broadcast_to(total_low[at].astype(F32), read.shape),
                ],
                axis=0,
            ).astype(BF16)
            pick = (
                take == (put // per_group) * heads + g * per_group + put % per_group
            ).astype(BF16)
            key_ref[g * seqs + i, span:, :] = jnp.dot(
                pick, stacked, preferred_element_type=F32
            ).astype(BF16)


def finish(x, other, begun, query, bias, gain):
    seqs, _, width = query.shape
    hd = gain.shape[0]
    span = x.shape[1] // seqs
    blocks = (width // hd) * seqs
    here = pl.BlockSpec(memory_space=pltpu.VMEM)
    return pl.pallas_call(
        finish_kernel,
        out_shape=(
            pltpu.VMEM((blocks, span + EXTRA, hd), BF16),
            pltpu.VMEM((blocks, span, hd), BF16),
        ),
        in_specs=[here, here, here, here, pl.BlockSpec(memory_space=pltpu.SMEM), here],
        compiler_params=vmem(24),
        name="finish",
    )(*on_chip(x, other, begun, query), bias, gain.reshape(1, hd))


def join_first_kernel(rows_ref, out_ref):
    count = rows_ref.shape[0]
    shape = (2, rows_ref.shape[2])
    read, log_later = jnp.zeros(shape, F32), jnp.zeros(shape, F32)
    for n in reversed(range(count)):
        rows = rows_ref[n, rows_ref.shape[1] - EXTRA :].astype(F32)
        read += jnp.exp(log_later) * (rows[0:2] + rows[2:4])
        log_later += rows[4:6] + rows[6:8]
    out_ref[0:2] = read
    out_ref[2:4] = log_later


def join_last_kernel(rows_ref, out_ref):
    count = rows_ref.shape[0]
    shape = (2, rows_ref.shape[2])
    read, log_later = jnp.zeros(shape, F32), jnp.zeros(shape, F32)
    for n in reversed(range(count)):
        read += jnp.exp(log_later) * rows_ref[n, 0:2]
        log_later += rows_ref[n, 2:4]
    out_ref[...] = read


def join_first(received):
    return pl.pallas_call(
        join_first_kernel,
        out_shape=pltpu.VMEM((4, received.shape[2]), F32),
        compiler_params=vmem(8),
        name="join_first",
    )(*on_chip(received))


def join_last(pieces):
    return pl.pallas_call(
        join_last_kernel,
        out_shape=jax.ShapeDtypeStruct((2, pieces.shape[2]), F32),
        compiler_params=vmem(4),
        name="join_last",
    )(*on_chip(pieces))


def shards(tokens, in_gain, w_key, w_value, k_gain, new_query, q_gain, stick_bias):
    seq_count, tok_seq, model_width = tokens.shape
    head_dim = k_gain.shape[0]
    heads = stick_bias.shape[0]
    kv_heads = w_key.shape[1] // head_dim
    per_group = heads // kv_heads
    pieces = along_z(w_key, w_value)
    kept, sent = norm_halves(tokens, in_gain)
    own = lax.all_to_all(spread(pieces, lax.axis_size(SP)), SP, 0, 0, tiled=True)
    own = own.reshape(2, model_width // 2, w_key.shape[1])
    came = lax.ppermute(sent, "c", [(0, 1), (1, 0)])
    x, query = arrange(kept, came, new_query, q_gain, kv_heads)
    x = x.reshape(2, seq_count * tok_seq, model_width // 2)
    other = lax.ppermute(own, "c", [(0, 1), (1, 0)])
    begun = partial_product(x, own)
    keys, values = finish(x, other, begun, query, stick_bias, k_gain)
    got_keys = lax.all_to_all(keys, "z", 0, 0, tiled=True)
    got_values = lax.all_to_all(values, "z", 0, 0, tiled=True)
    joined = join_first(got_keys)
    everything = lax.all_gather(joined, SP)
    read = join_last(everything)
    span = 2 * tok_seq
    positions = got_keys.shape[0] * span
    key_cache = got_keys[:, :span].reshape(1, positions, head_dim)
    value_cache = got_values.reshape(1, positions, head_dim)
    return (key_cache, value_cache, read.reshape(1, per_group * head_dim))


def solution(mesh):
    grid = Mesh(mesh.devices.reshape(4, 4, 16, 2), ("y", "x", "z", "c"))
    tp = ("z", "c")
    return jax.shard_map(
        shards,
        mesh=grid,
        in_specs=(
            P(None, ("y", "x", "z", "c"), None),
            P(),
            P(tp, None),
            P(tp, None),
            P(),
            P(),
            P(),
            P(),
        ),
        out_specs=(P(tp, SP, None), P(tp, SP, None), P(tp, None)),
        check_vma=False,
    )
```

time: 190 us -> 206 us (1.084)
  the two profiles are of different devices: /device:TPU:1 before, /device:TPU:32 now
where the time goes in v2:
time: 206 us
  blocking collectives  131 us (64%)
  waiting for transfers between devices  44.2 us (21%)
  Pallas kernels  17.3 us (8%)
  starting transfers between devices  10.6 us (5%)
    all_to_all x1, blocking collectives, shards(): got_values = lax.all_to_all(values, 'z', 0, 0, tiled=True)  47.5 us
    all_to_all x1, waiting for transfers between devices, shards(): got_keys = lax.all_to_all(keys, 'z', 0, 0, tiled=True)  41.1 us
    all_to_all x1, blocking collectives, shards(): lax.all_to_all(spread(pieces, lax.axis_size(SP)), SP, 0, 0, tiled=True)  32.7 us
    all_to_all x1, blocking collectives, to_all(): lax.all_to_all(jnp.broadcast_to(piece[None], (count, *piece.shape)), axis...  29.2 us
    all_gather x1, blocking collectives, shards(): everything = lax.all_gather(joined, SP)  21.2 us
    pallas_call x1, Pallas kernels, finish(): pl.pallas_call(finish_kernel, out_shape=(pltpu.VMEM((blocks, span + EXTRA...  6.69 us
    pallas_call x1, Pallas kernels, arrange(): pl.pallas_call(arrange_kernel, out_shape=(pltpu.VMEM((2, 2, seqs * length...  6.66 us
    all_to_all x1, starting transfers between devices, shards(): got_keys = lax.all_to_all(keys, 'z', 0, 0, tiled=True)  6.11 us
  transfers between devices with their start and end apart: 3, of which 2 were waited for; matrix products, arithmetic and copies ran while one was open for 0% of the time, Pallas kernels for 5%

profile of v2, /device:TPU:32, one launch (start us, length us, event | category | flops | bytes accessed | tf_op | source)
XLA Modules:
  0.0 205.9 jit_solution(10565705414451429549)
XLA Ops:
  0.7 0.7 dynamic-slice_select_fusion
  1.4 29.2 %all_to_all.20.piece_ref = bf16[16,8,512]{2,1,0:T(8,128)(2,1)S(1)} all-to-all(bf16[16,8,512]{2,1,0:T(8,128)(2,1)S(1)} %broadcast_in_dim.2), channel_id=1, replica_groups=mesh['y'=4,'x'=4,'z'=16,'c'=2] {'z'}, dimensions={0} | all-to-all | bytes 262144 | tf_op jit(solution)/shard_map/all_to_all | solution.py:23
  30.6 0.2 spread.1
  30.8 0.0 copy-start
  30.8 0.0 copy-start.2
  30.8 32.7 %all_to_all.21 = bf16[16,16,8,512]{3,2,1,0:T(8,128)(2,1)S(1)} all-to-all(bf16[16,16,8,512]{3,2,1,0:T(8,128)(2,1)S(1)} %spread.1), channel_id=1, replica_groups=mesh['y'=4,'x'=4,'z'=16,'c'=2] {'y','x'}, dimensions={0} | all-to-all | bytes 4194304 | tf_op jit(solution)/shard_map/all_to_all | solution.py:318
  63.5 2.0 collective-permute-start.1
  65.6 0.0 copy-done
  65.6 1.3 norm_halves.1
  66.9 2.4 %collective-permute-start = (bf16[4,96,2048]{2,1,0:T(8,128)(2,1)S(1)}, bf16[4,96,2048]{2,1,0:T(8,128)(2,1)S(1)}, u32[]{:S(2)}, u32[]{:S(2)}) collective-permute-start(bf16[4,96,2048]{2,1,0:T(8,128)(2,1)S(1)} %get-tuple-element.10), channel_id=1, source_target_pairs={{0,1},{1,0},{2,3},{3,2},{4,5},{5,4},{6,7},{7,6},{8,9},{9,8},{10,11... | collective-permute-start | bytes 4718600 | tf_op jit(solution)/shard_map/ppermute | solution.py:320
  69.3 3.0 %collective-permute-done.came_ref = bf16[4,96,2048]{2,1,0:T(8,128)(2,1)S(1)} collective-permute-done((bf16[4,96,2048]{2,1,0:T(8,128)(2,1)S(1)}, bf16[4,96,2048]{2,1,0:T(8,128)(2,1)S(1)}, u32[]{:S(2)}, u32[]{:S(2)}) %collective-permute-start) | collective-permute-done | bytes 1572896 | tf_op jit(solution)/shard_map/ppermute | solution.py:320
  72.4 6.7 %arrange.1 = (bf16[2,2,384,1024]{3,2,1,0:T(8,128)(2,1)S(1)}, bf16[4,8,512]{2,1,0:T(8,128)(2,1)S(1)}) custom-call(bf16[4,96,2048]{2,1,0:T(8,128)(2,1)S(1)} %get-tuple-element.9.kept_ref, bf16[4,96,2048]{2,1,0:T(8,128)(2,1)S(1)} %collective-permute-done.came_ref, bf16[8,1024]{1,0:T(8,128)(2,1)S(1)} %copy-done.1, f32[1,128]{1,0:T(1,128)S(1)} %bitcast.16), custom_call_target="tpu_custom_call" | custom-call | tf_op jit(solution)/shard_map/arrange/pallas_call | solution.py:139
  79.0 0.0 copy-start.3
  79.0 0.0 copy-start.4
  79.0 1.8 partial.1.begun_ref
  80.8 0.0 collective-permute-done.1.rows_ref
  80.9 6.7 %finish.1 = (bf16[16,200,128]{2,1,0:T(8,128)(2,1)}, bf16[16,192,128]{2,1,0:T(8,128)(2,1)S(1)}) custom-call(bf16[2,768,1024]{2,1,0:T(8,128)(2,1)S(1)} %bitcast.10, bf16[2,1024,512]{2,1,0:T(8,128)(2,1)S(1)} %collective-permute-done.1.rows_ref, f32[2,768,512]{2,1,0:T(8,128)S(1)} %partial.1.begun_ref, bf16[4,8,512]{2,1,0:T(8,128)(2,1)S(1)} %get-tuple-element.12.query_ref, ...), custom_call_target="tpu_custom_call" | custom-call | tf_op jit(solution)/shard_map/finish/pallas_call | solution.py:258
  87.6 47.5 %all_to_all.22 = bf16[16,192,128]{2,1,0:T(8,128)(2,1)S(1)} all-to-all(bf16[16,192,128]{2,1,0:T(8,128)(2,1)S(1)} %get-tuple-element.14), channel_id=1, replica_groups=mesh['y'=4,'x'=4,'z'=16,'c'=2] {'z'}, dimensions={0} | all-to-all | bytes 1572864 | tf_op jit(solution)/shard_map/all_to_all | solution.py:327
  135.0 6.1 %all-to-all-start.2 = ((bf16[16,200,128]{2,1,0:T(8,128)(2,1)}), bf16[16,200,128]{2,1,0:T(8,128)(2,1)S(1)}, u32[]{:S(2)}, u32[]{:S(2)}) async-start(bf16[16,200,128]{2,1,0:T(8,128)(2,1)} %get-tuple-element.13), calls=%async_computation.2 | async-start | bytes 1638400 | tf_op jit(solution)/shard_map/all_to_all | solution.py:326
  141.1 41.1 %all-to-all-done.2.rows_ref = bf16[16,200,128]{2,1,0:T(8,128)(2,1)S(1)} async-done(((bf16[16,200,128]{2,1,0:T(8,128)(2,1)}), bf16[16,200,128]{2,1,0:T(8,128)(2,1)S(1)}, u32[]{:S(2)}, u32[]{:S(2)}) %all-to-all-start.2) | async-done | bytes 819232 | tf_op jit(solution)/shard_map/all_to_all | solution.py:326
  182.3 21.2 %all-gather.1.rows_ref = f32[16,4,128]{2,1,0:T(4,128)S(1)} all-gather(f32[1,4,128]{2,1,0:T(4,128)S(1)} %bitcast.14), channel_id=2, replica_groups=mesh['y'=4,'x'=4,'z'=16,'c'=2] {'y','x'}, dimensions={0}, use_global_device_ids=true | all-gather | bytes 34816 | tf_op jit(solution)/shard_map/all_gather | solution.py:329
  203.5 0.6 join_last.1
  204.1 1.0 slice.4
  205.0 0.9 copy.12
  (9 shorter events, 0.1 us)
Async XLA Ops:
  30.8 34.8 %copy-start = (bf16[8,96,2048]{2,1,0:T(8,128)(2,1)S(1)}, bf16[8,96,2048]{2,1,0:T(8,128)(2,1)}, u32[]{:S(2)}) copy-start(bf16[8,96,2048]{2,1,0:T(8,128)(2,1)} %tokens_ref.1) | copy-start | bytes 9437188
  30.8 34.8 %copy-start.2 = (f32[2048]{0:T(1024)S(1)}, f32[2048]{0:T(1024)}, u32[]{:S(2)}) copy-start(f32[2048]{0:T(1024)} %param.9) | copy-start | bytes 24580
  63.5 8.8 %copy-start.1 = (bf16[8,1024]{1,0:T(8,128)(2,1)S(1)}, bf16[8,1024]{1,0:T(8,128)(2,1)}, u32[]{:S(2)}) copy-start(bf16[8,1024]{1,0:T(8,128)(2,1)} %query_ref.1) | copy-start | bytes 49156
  63.5 8.8 %copy-start.5 = (f32[128]{0:T(128)S(1)}, f32[128]{0:T(128)}, u32[]{:S(2)}) copy-start(f32[128]{0:T(128)} %param.14) | copy-start | bytes 1540
  63.5 17.3 %collective-permute-start.1 = (bf16[2,1024,512]{2,1,0:T(8,128)(2,1)S(1)}, bf16[2,1024,512]{2,1,0:T(8,128)(2,1)S(1)}, u32[]{:S(2)}, u32[]{:S(2)}) collective-permute-start(bf16[2,1024,512]{2,1,0:T(8,128)(2,1)S(1)} %bitcast.11), channel_id=1, source_target_pairs={{0,1},{1,0},{2,3},{3,2},{4,5},{5,4},{6,7},{7,6},{8,9},{9,8},{10,11... | collective-permute-start | bytes 6291464 | tf_op jit(solution)/shard_map/ppermute | solution.py:323
  66.9 5.4 %collective-permute-start = (bf16[4,96,2048]{2,1,0:T(8,128)(2,1)S(1)}, bf16[4,96,2048]{2,1,0:T(8,128)(2,1)S(1)}, u32[]{:S(2)}, u32[]{:S(2)}) collective-permute-start(bf16[4,96,2048]{2,1,0:T(8,128)(2,1)S(1)} %get-tuple-element.10), channel_id=1, source_target_pairs={{0,1},{1,0},{2,3},{3,2},{4,5},{5,4},{6,7},{7,6},{8,9},{9,8},{10,11... | collective-permute-start | bytes 4718600 | tf_op jit(solution)/shard_map/ppermute | solution.py:320
  79.0 1.8 copy-start.3
  79.0 1.8 copy-start.4
  135.0 47.3 %all-to-all-start.2 = ((bf16[16,200,128]{2,1,0:T(8,128)(2,1)}), bf16[16,200,128]{2,1,0:T(8,128)(2,1)S(1)}, u32[]{:S(2)}, u32[]{:S(2)}) async-start(bf16[16,200,128]{2,1,0:T(8,128)(2,1)} %get-tuple-element.13), calls=%async_computation.2 | async-start | bytes 1638400 | tf_op jit(solution)/shard_map/all_to_all | solution.py:326

commit v3 on v2

v3 whole, which is shorter than its diff:
```python
import functools

import jax
import jax.numpy as jnp
from jax import lax
from jax.experimental import pallas as pl
from jax.experimental.pallas import tpu as pltpu
from jax.sharding import Mesh
from jax.sharding import PartitionSpec as P

NORM_EPS = 1e-06
SP = ("y", "x")
EXTRA = 8
F32 = jnp.float32
BF16 = jnp.bfloat16


def root_norm(values, scaling):
    inverse = lax.rsqrt(jnp.mean(values * values, axis=-1, keepdims=True) + NORM_EPS)
    return values * inverse * scaling


def to_all(piece, axis):
    count = lax.axis_size(axis)
    return lax.all_to_all(
        jnp.broadcast_to(piece[None], (count, *piece.shape)), axis, 0, 0, tiled=True
    )


def along_z(w_key, w_value):
    rows = w_key.shape[0] // lax.axis_size("x")
    width = w_key.shape[1] // lax.axis_size("y")
    at = (lax.axis_index("x") * rows, lax.axis_index("y") * width)
    parts = [lax.dynamic_slice(w, at, (rows, width)) for w in (w_key, w_value)]
    return to_all(jnp.stack(parts), "z")


def norm_kernel(tokens_ref, gain_ref, kept_ref, sent_ref):
    core = lax.axis_index("c")
    gain = gain_ref[...]
    kept_ref[0] = root_norm(tokens_ref[core].astype(F32), gain).astype(BF16)
    sent_ref[0] = root_norm(tokens_ref[1 - core].astype(F32), gain).astype(BF16)


def norm_halves(tokens, in_gain):
    seq_count, length, model = tokens.shape
    half = pltpu.HBM((seq_count // 2, length, model), BF16)
    block = pl.BlockSpec((1, length, model), lambda i: (i, 0, 0))
    return pl.pallas_call(
        norm_kernel,
        grid=(seq_count // 2,),
        out_shape=(half, half),
        in_specs=[
            pl.BlockSpec((2, length, model), lambda i: (i, 0, 0)),
            pl.BlockSpec((1, model), lambda i: (0, 0)),
        ],
        out_specs=(block, block),
        compiler_params=vmem(16),
        name="norm_halves",
    )(*off_chip(tokens, in_gain.reshape(1, model)))


def spread_kernel(pieces_ref, early_ref, late_ref):
    zs = pieces_ref.shape[0]
    early = early_ref.shape[1] - zs
    for n in range(early_ref.shape[0]):
        early_ref[n, :zs] = pieces_ref[:, 0]
        early_ref[n, zs:] = pieces_ref[:early, 1]
    late_ref[...] = pieces_ref[early:, 1]


def spread(pieces, count):
    zs, _, rows, width = pieces.shape
    early = zs // 8
    return pl.pallas_call(
        spread_kernel,
        out_shape=(
            jax.ShapeDtypeStruct((count, zs + early, rows, width), pieces.dtype),
            jax.ShapeDtypeStruct((zs - early, rows, width), pieces.dtype),
        ),
        compiler_params=vmem(8),
        name="spread",
    )(*on_chip(pieces))


def vmem(mib):
    return pltpu.CompilerParams(vmem_limit_bytes=mib * 1024 * 1024)


def on_chip(*arrays):
    return tuple(pltpu.with_memory_space_constraint(a, pltpu.VMEM) for a in arrays)


def off_chip(*arrays):
    return tuple(pltpu.with_memory_space_constraint(a, pltpu.HBM) for a in arrays)


def high_low(values):
    high = values.astype(BF16)
    return high, (values - high.astype(F32)).astype(BF16)


def arrange_kernel(
    kept_hbm, came_hbm, query_ref, gain_ref, x_ref, grouped_ref, kept_ref, came_ref, sems
):
    core = lax.axis_index("c")
    loads = [
        pltpu.make_async_copy(kept_hbm, kept_ref, sems.at[0]),
        pltpu.make_async_copy(came_hbm, came_ref, sems.at[1]),
    ]
    for load in loads:
        load.start()
    seqs, length, model = kept_ref.shape
    hd = gain_ref.shape[1]
    heads = query_ref.shape[1] // hd
    kv_heads = grouped_ref.shape[2] // hd
    zs, xs = lax.axis_size("z"), lax.axis_size("x")
    held = model // zs // 2
    rows = held // xs
    part = hd // rows
    deep = part * 2 * held
    source = lax.broadcasted_iota(jnp.int32, (deep, 2 * hd), 0)
    column = lax.broadcasted_iota(jnp.int32, (deep, 2 * hd), 1)
    inside = column % hd
    offset = source - (inside // rows) * (2 * held) - inside % rows - (column // hd) * rows

    query = query_ref[...].astype(F32)
    row = lax.broadcasted_iota(jnp.int32, (heads, hd), 0)
    per_group = heads // kv_heads
    for i in range(seqs):
        mine = jnp.where(core == 0, query[2 * i : 2 * i + 1], query[2 * i + 1 : 2 * i + 2])
        for g in range(kv_heads):
            block = jnp.zeros((heads, hd), F32)
            for j in range(g * per_group, (g + 1) * per_group):
                head = root_norm(mine[:, j * hd : (j + 1) * hd], gain_ref[...])
                block = jnp.where(row == j, head, block)
            grouped_ref[i, :, g * hd : (g + 1) * hd] = block.astype(BF16)
    for load in loads:
        load.wait()
    kept = kept_ref[...].reshape(seqs * length, model)
    came = came_ref[...].reshape(seqs * length, model)
    for half in range(2):
        for r in range(0, xs, 2):
            pick = (offset == half * held + r * rows).astype(BF16)
            for n in range(zs // part):
                for values, at in ((kept, core), (came, 1 - core)):
                    moved = jnp.dot(
                        values[:, n * deep : (n + 1) * deep], pick, preferred_element_type=F32
                    ).astype(BF16)
                    for k in range(2):
                        start = (r + k) * zs * rows + n * hd
                        x_ref[half, at, :, start : start + hd] = moved[:, k * hd : (k + 1) * hd]


def arrange(kept, came, new_query, q_gain, kv_heads):
    seqs, length, model = kept.shape
    hd = q_gain.shape[0]
    heads = new_query.shape[1] // hd
    return pl.pallas_call(
        arrange_kernel,
        out_shape=(
            pltpu.VMEM((2, 2, seqs * length, model // 2), BF16),
            pltpu.VMEM((seqs, heads, kv_heads * hd), BF16),
        ),
        in_specs=[pl.BlockSpec(memory_space=pl.ANY)] * 2
        + [pl.BlockSpec(memory_space=pltpu.VMEM)] * 2,
        scratch_shapes=[
            pltpu.VMEM(kept.shape, BF16),
            pltpu.VMEM(kept.shape, BF16),
            pltpu.SemaphoreType.DMA((2,)),
        ],
        compiler_params=vmem(32),
        name="arrange",
    )(*off_chip(kept), came, new_query, q_gain.reshape(1, hd))


def two_heads(refs, head):
    columns = []
    for g in (head, head + 1):
        blocks = [ref[g, n, first:last] for n in range(refs[0][0].shape[1]) for ref, first, last in refs]
        columns.append(jnp.concatenate(blocks, axis=0))
    return jnp.concatenate(columns, axis=1)


def key_part(early_ref, held):
    return ((early_ref, 0, held),)


def value_parts(early_ref, late_ref, held):
    first = held if early_ref.shape[2] > held else 0
    return ((early_ref, first, early_ref.shape[2]), (late_ref, 0, late_ref.shape[2]))


def partial_kernel(*refs):
    x_ref, *rows_refs, out_ref = refs
    x = x_ref[lax.axis_index("c")]
    heads, count, _, hd = rows_refs[0].shape
    held = x.shape[1] // count
    parts = key_part(*rows_refs, held) if len(rows_refs) == 1 else value_parts(*rows_refs, held)
    for g in range(0, heads, 2):
        out_ref[:, g * hd : (g + 2) * hd] = jnp.dot(
            x, two_heads(parts, g), preferred_element_type=F32
        )


def partial_product(x, rows):
    width = rows[0].shape[0] * rows[0].shape[-1]
    return pl.pallas_call(
        partial_kernel,
        out_shape=pltpu.VMEM((x.shape[1], width), F32),
        compiler_params=vmem(16),
        name="partial",
    )(*on_chip(x), *rows)


def place(ref, seqs, length, g, head):
    for n in range(2 * seqs):
        h, i = divmod(n, seqs)
        ref[g * seqs + i, h * length : (h + 1) * length, :] = head[n * length : (n + 1) * length]


def keys_kernel(x_ref, rows_ref, begun_ref, gain_ref, key_ref, rest_ref):
    x = x_ref[1 - lax.axis_index("c")]
    gain = gain_ref[...]
    kv_heads, hd = rows_ref.shape[0], gain.shape[1]
    held = x.shape[1] // rows_ref.shape[1]
    seqs = key_ref.shape[0] // kv_heads
    for g in range(0, kv_heads, 2):
        raw = begun_ref[:, g * hd : (g + 2) * hd] + jnp.dot(
            x, two_heads(key_part(rows_ref, held), g), preferred_element_type=F32
        )
        for k in range(2):
            head = root_norm(raw[:, k * hd : (k + 1) * hd], gain).astype(BF16)
            place(key_ref, seqs, key_ref.shape[1] // 2, g + k, head)
    rest_ref[...] = rows_ref[:, :, held:]


def make_keys(x, other, begun, gain, seqs):
    kv_heads, parts, rows, hd = other.shape
    rest = rows - x.shape[2] // parts
    return pl.pallas_call(
        keys_kernel,
        out_shape=(
            pltpu.HBM((kv_heads * seqs, x.shape[1] // seqs, hd), BF16),
            pltpu.HBM((kv_heads, parts, rest, hd), BF16),
        ),
        compiler_params=vmem(16),
        name="make_keys",
    )(*on_chip(x, other, begun), gain.reshape(1, hd))


def values_kernel(x_ref, early_ref, late_ref, begun_ref, key_ref, query_ref, bias_ref, value_ref):
    core = lax.axis_index("c")
    seqs, heads, width = query_ref.shape
    hd = key_ref.shape[2]
    span = key_ref.shape[1]
    kv_heads = width // hd
    per_group = heads // kv_heads
    x = x_ref[1 - core]
    held = x.shape[1] // early_ref.shape[1]

    row = lax.broadcasted_iota(jnp.int32, (heads, 1), 0)
    bias = jnp.zeros((heads, 1), F32)
    for j in range(heads):
        bias = jnp.where(row == j, bias_ref[j], bias)
    scores = []
    for i in range(seqs):
        total = jnp.zeros((heads, span), F32)
        for g in range(kv_heads):
            total += lax.dot_general(
                query_ref[i, :, g * hd : (g + 1) * hd],
                key_ref[g * seqs + i],
                (((1,), (1,)), ((), ())),
                preferred_element_type=F32,
            )
        scores.append(total * (hd**-0.5) + bias)
    scores = jnp.concatenate(scores, axis=0)
    log_keep = -(jnp.maximum(scores, 0.0) + jnp.log1p(jnp.exp(-jnp.abs(scores))))
    first = lax.broadcasted_iota(jnp.int32, (span, span), 0)
    second = lax.broadcasted_iota(jnp.int32, (span, span), 1)
    later = (first > second).astype(BF16)
    after = jnp.zeros(scores.shape, F32)
    rest = log_keep
    for _ in range(3):
        part = rest.astype(BF16)
        rest = rest - part.astype(F32)
        after += jnp.dot(part, later, preferred_element_type=F32)
    weight_high, weight_low = high_low(jnp.exp(scores + log_keep + after))
    total_high, total_low = high_low(jnp.sum(log_keep, axis=1, keepdims=True))

    for g in range(0, kv_heads, 2):
        raw = begun_ref[:, g * hd : (g + 2) * hd] + jnp.dot(
            x, two_heads(value_parts(early_ref, late_ref, held), g), preferred_element_type=F32
        )
        for k in range(2):
            place(value_ref, seqs, span // 2, g + k, raw[:, k * hd : (k + 1) * hd].astype(BF16))

    put = lax.broadcasted_iota(jnp.int32, (EXTRA, 4 * heads), 0)
    take = lax.broadcasted_iota(jnp.int32, (EXTRA, 4 * heads), 1)
    for i in range(seqs):
        at = slice(i * heads, (i + 1) * heads)
        for g in range(kv_heads):
            values = value_ref[g * seqs + i, 0:span]
            read = jnp.dot(weight_high[at], values, preferred_element_type=F32) + jnp.dot(
                weight_low[at], values, preferred_element_type=F32
            )
            read_high, read_low = high_low(read)
            stacked = jnp.concatenate(
                [
                    read_high.astype(F32),
                    read_low.astype(F32),
                    jnp.broadcast_to(total_high[at].astype(F32), read.shape),
                    jnp.broadcast_to(total_low[at].astype(F32), read.shape),
                ],
                axis=0,
            ).astype(BF16)
            pick = (
                take == (put // per_group) * heads + g * per_group + put % per_group
            ).astype(BF16)
            value_ref[g * seqs + i, span:, :] = jnp.dot(
                pick, stacked, preferred_element_type=F32
            ).astype(BF16)


def make_values(x, others, begun, keys, query, bias):
    blocks, span, hd = keys.shape
    here = pl.BlockSpec(memory_space=pltpu.VMEM)
    return pl.pallas_call(
        values_kernel,
        out_shape=pltpu.HBM((blocks, span + EXTRA, hd), BF16),
        in_specs=[here] * 6 + [pl.BlockSpec(memory_space=pltpu.SMEM)],
        compiler_params=vmem(24),
        name="make_values",
    )(*on_chip(x), others[0], *on_chip(others[1], begun), keys, *on_chip(query), bias)


def store_kernel(rows_ref, out_ref, sem):
    copy = pltpu.make_async_copy(rows_ref, out_ref, sem)
    copy.start()
    copy.wait()


def store(rows):
    return pl.pallas_call(
        store_kernel,
        out_shape=pltpu.HBM(rows.shape, rows.dtype),
        in_specs=[pl.BlockSpec(memory_space=pl.ANY)],
        out_specs=pl.BlockSpec(memory_space=pl.ANY),
        scratch_shapes=[pltpu.SemaphoreType.DMA],
        compiler_params=vmem(4),
        name="store",
    )(rows)


def join_first_kernel(rows_ref, out_ref):
    count = rows_ref.shape[0]
    shape = (2, rows_ref.shape[2])
    read, log_later = jnp.zeros(shape, F32), jnp.zeros(shape, F32)
    for n in reversed(range(count)):
        rows = rows_ref[n, rows_ref.shape[1] - EXTRA :].astype(F32)
        read += jnp.exp(log_later) * (rows[0:2] + rows[2:4])
        log_later += rows[4:6] + rows[6:8]
    for n in range(out_ref.shape[0]):
        out_ref[n, 0:2] = read
        out_ref[n, 2:4] = log_later


def join_last_kernel(rows_ref, out_ref):
    count = rows_ref.shape[0]
    shape = (2, rows_ref.shape[2])
    read, log_later = jnp.zeros(shape, F32), jnp.zeros(shape, F32)
    for n in reversed(range(count)):
        read += jnp.exp(log_later) * rows_ref[n, 0:2]
        log_later += rows_ref[n, 2:4]
    out_ref[...] = read


def join_first(received, copies):
    return pl.pallas_call(
        join_first_kernel,
        out_shape=jax.ShapeDtypeStruct((copies, 4, received.shape[2]), F32),
        compiler_params=vmem(8),
        name="join_first",
    )(*on_chip(received))


def join_last(pieces):
    return pl.pallas_call(
        join_last_kernel,
        out_shape=jax.ShapeDtypeStruct((2, pieces.shape[2]), F32),
        compiler_params=vmem(4),
        name="join_last",
    )(*on_chip(pieces))


def shards(tokens, in_gain, w_key, w_value, k_gain, new_query, q_gain, stick_bias):
    seq_count, tok_seq, model_width = tokens.shape
    head_dim = k_gain.shape[0]
    heads = stick_bias.shape[0]
    kv_heads = w_key.shape[1] // head_dim
    per_group = heads // kv_heads
    seqs = seq_count // 2
    trade = functools.partial(lax.ppermute, axis_name="c", perm=[(0, 1), (1, 0)])
    ys, xs = lax.axis_size("y"), lax.axis_size("x")
    pieces = along_z(w_key, w_value)
    kept, sent = norm_halves(tokens, in_gain)
    early, late = spread(pieces, ys * xs)
    came = trade(sent)
    early = lax.all_to_all(early, SP, 0, 0, tiled=True)
    x, query = arrange(kept, came, new_query, q_gain, kv_heads)
    x = x.reshape(2, seq_count * tok_seq, model_width // 2)
    early = early.reshape(ys, xs, -1, head_dim)
    early_other = trade(early)
    begun = partial_product(x, (early,))
    keys, early_other = make_keys(x, early_other, begun, k_gain, seqs)
    got_keys = lax.all_to_all(keys, "z", 0, 0, tiled=True)
    late = lax.all_gather(late, SP).reshape(ys, xs, -1, head_dim)
    late_other = trade(late)
    begun = partial_product(x, (early, late))
    values = make_values(x, (early_other, late_other), begun, keys, query, stick_bias)
    got_values = lax.all_to_all(values, "z", 0, 0, tiled=True)
    stored = store(got_keys)
    joined = join_first(got_values, ys * xs)
    everything = lax.all_to_all(joined, SP, 0, 0, tiled=True)
    read = join_last(everything)
    span = 2 * tok_seq
    positions = got_keys.shape[0] * span
    key_cache = stored.reshape(1, positions, head_dim)
    value_cache = got_values[:, :span].reshape(1, positions, head_dim)
    return (key_cache, value_cache, read.reshape(1, per_group * head_dim))


def solution(mesh):
    grid = Mesh(mesh.devices.reshape(4, 4, 16, 2), ("y", "x", "z", "c"))
    tp = ("z", "c")
    return jax.shard_map(
        shards,
        mesh=grid,
        in_specs=(
            P(None, ("y", "x", "z", "c"), None),
            P(),
            P(tp, None),
            P(tp, None),
            P(),
            P(),
            P(),
            P(),
        ),
        out_specs=(P(tp, SP, None), P(tp, SP, None), P(tp, None)),
        check_vma=False,
    )
```

time: 206 us -> 206 us (level)
  blocking collectives: 131 us -> 100 us
  starting transfers between devices: 10.6 us -> 24.4 us
  waiting for transfers between devices: 44.2 us -> 54.7 us
  Pallas kernels: 17.3 us -> 23.1 us
    all_to_all x1 -> x0, blocking collectives: 32.7 us -> none  [shards(): lax.all_to_all(spread(pieces, lax.axis_size(SP)), SP, 0, 0, tiled=True)]
    all_to_all x0 -> x2, waiting for transfers between devices: none -> 15.5 us  [the longest x1 9.74 us: shards(): early = lax.all_to_all(early, SP, 0, 0, tiled=True)]
    all_to_all x0 -> x2, starting transfers between devices: none -> 12 us  [the longest x1 7.03 us: shards(): early = lax.all_to_all(early, SP, 0, 0, tiled=True)]
    pallas_call x4 -> x7, Pallas kernels: 8.7 us -> 13 us  [the longest x1 6.18 us: make_values(): pl.pallas_call(values_kernel, out_shape=pltpu.HBM((blocks, span + EXTRA,...]
    pallas_call x1, Pallas kernels: 1.32 us -> 4.61 us  [norm_halves(): pl.pallas_call(norm_kernel, grid=(seq_count // 2,), out_shape=(half, half...]
    ppermute x2 -> x3, waiting for transfers between devices: 3.02 us -> 0.01 us  [the longest x1 0.01 us: shards(): came = trade(sent)]
    ppermute x2 -> x3, starting transfers between devices: 4.45 us -> 5.73 us  [the longest x1 1.91 us: shards(): late_other = trade(late)]
  transfers between devices with their start and end apart: 3 -> 6, of which waited for: 2 -> 3; matrix products, arithmetic and copies ran while one was open for 0% -> 0% of each run, Pallas kernels for 5% -> 7%
where the time goes in v3:
time: 206 us
  blocking collectives  100 us (49%)
  waiting for transfers between devices  54.7 us (27%)
  starting transfers between devices  24.4 us (12%)
  Pallas kernels  23.1 us (11%)
  local copies, waits for them, and re-layouts  2.62 us (1%)
    all_to_all x1, blocking collectives, shards(): got_values = lax.all_to_all(values, 'z', 0, 0, tiled=True)  47.9 us
    all_to_all x1, waiting for transfers between devices, shards(): got_keys = lax.all_to_all(keys, 'z', 0, 0, tiled=True)  39.2 us
    all_to_all x1, blocking collectives, to_all(): lax.all_to_all(jnp.broadcast_to(piece[None], (count, *piece.shape)), axis...  29.2 us
    all_gather x1, blocking collectives, shards(): late = lax.all_gather(late, SP).reshape(ys, xs, -1, head_dim)  22.9 us
    all_to_all x1, waiting for transfers between devices, shards(): early = lax.all_to_all(early, SP, 0, 0, tiled=True)  9.74 us
    all_to_all x1, starting transfers between devices, shards(): early = lax.all_to_all(early, SP, 0, 0, tiled=True)  7.03 us
    all_to_all x1, starting transfers between devices, shards(): got_keys = lax.all_to_all(keys, 'z', 0, 0, tiled=True)  6.73 us
    pallas_call x1, Pallas kernels, make_values(): pl.pallas_call(values_kernel, out_shape=pltpu.HBM((blocks, span + EXTRA,...  6.18 us
  transfers between devices with their start and end apart: 6, of which 3 were waited for; matrix products, arithmetic and copies ran while one was open for 0% of the time, Pallas kernels for 7%

profile of v3, /device:TPU:32, one launch (start us, length us, event | category | flops | bytes accessed | tf_op | source)
XLA Modules:
  0.0 205.6 jit_solution(6970803039560082420)
XLA Ops:
  0.6 0.7 dynamic-slice_bitcast_fusion
  1.4 29.2 %all_to_all.25.pieces_ref = bf16[16,2,16,128]{3,2,1,0:T(8,128)(2,1)S(1)} all-to-all(bf16[16,2,16,128]{3,2,1,0:T(8,128)(2,1)S(1)} %broadcast_in_dim.2), channel_id=1, replica_groups=mesh['y'=4,'x'=4,'z'=16,'c'=2] {'z'}, dimensions={0} | all-to-all | bytes 262144 | tf_op jit(solution)/shard_map/all_to_all | solution.py:25
  30.6 1.2 spread.1
  31.8 7.0 %all-to-all-start.1 = ((bf16[16,18,16,128]{3,2,1,0:T(8,128)(2,1)}), bf16[16,18,16,128]{3,2,1,0:T(8,128)(2,1)S(1)}, u32[]{:S(2)}, u32[]{:S(2)}) async-start(bf16[16,18,16,128]{3,2,1,0:T(8,128)(2,1)} %get-tuple-element.14), calls=%async_computation.1 | async-start | bytes 2359296 | tf_op jit(solution)/shard_map/all_to_all | solution.py:409
  38.8 4.6 %norm_halves.1 = (bf16[4,96,2048]{2,1,0:T(8,128)(2,1)}, bf16[4,96,2048]{2,1,0:T(8,128)(2,1)}) custom-call(bf16[8,96,2048]{2,1,0:T(8,128)(2,1)} %tokens_ref.1, f32[1,2048]{1,0:T(1,128)} %bitcast.26), custom_call_target="tpu_custom_call" | custom-call | tf_op jit(solution)/shard_map/norm_halves/pallas_call | solution.py:49
  43.4 1.9 collective-permute-start
  45.4 9.7 %all-to-all-done.1 = bf16[16,18,16,128]{3,2,1,0:T(8,128)(2,1)S(1)} async-done(((bf16[16,18,16,128]{3,2,1,0:T(8,128)(2,1)}), bf16[16,18,16,128]{3,2,1,0:T(8,128)(2,1)S(1)}, u32[]{:S(2)}, u32[]{:S(2)}) %all-to-all-start.1) | async-done | bytes 1179680 | tf_op jit(solution)/shard_map/all_to_all | solution.py:409
  55.1 1.9 collective-permute-start.1
  57.0 22.9 %all-gather = bf16[224,16,128]{2,1,0:T(8,128)(2,1)S(1)} all-gather(bf16[14,16,128]{2,1,0:T(8,128)(2,1)S(1)} %get-tuple-element.17), channel_id=2, replica_groups=mesh['y'=4,'x'=4,'z'=16,'c'=2] {'y','x'}, dimensions={0}, use_global_device_ids=true | all-gather | bytes 974848 | tf_op jit(solution)/shard_map/all_gather | solution.py:417
  79.9 1.9 collective-permute-start.2
  81.9 4.9 %arrange.1 = (bf16[2,2,384,1024]{3,2,1,0:T(8,128)(2,1)S(1)}, bf16[4,8,512]{2,1,0:T(8,128)(2,1)S(1)}) custom-call(bf16[4,96,2048]{2,1,0:T(8,128)(2,1)} %get-tuple-element.11.kept_hbm, bf16[4,96,2048]{2,1,0:T(8,128)(2,1)S(1)} %collective-permute-done.came_hbm, bf16[8,1024]{1,0:T(8,128)(2,1)S(1)} %copy-done.1, f32[1,128]{1,0:T(1,128)S(1)} %bitcast.23), custom_call_target="tpu_custom_call" | custom-call | tf_op jit(solution)/shard_map/arrange/pallas_call | solution.py:159
  86.7 1.0 partial.2.begun_ref
  87.7 1.0 partial.3.begun_ref
  88.7 2.2 %make_keys.1 = (bf16[16,192,128]{2,1,0:T(8,128)(2,1)}, bf16[4,4,32,128]{3,2,1,0:T(8,128)(2,1)}) custom-call(bf16[2,768,1024]{2,1,0:T(8,128)(2,1)S(1)} %bitcast.15, bf16[4,4,288,128]{3,2,1,0:T(8,128)(2,1)S(1)} %collective-permute-done.1.rows_ref, f32[768,512]{1,0:T(8,128)S(1)} %partial.2.begun_ref, f32[1,128]{1,0:T(1,128)S(1)} %bitcast.22), custom_call_target="tpu_custom_call" | custom-call | tf_op jit(solution)/shard_map/make_keys/pallas_call | solution.py:241
  91.0 0.9 copy-done
  91.9 6.2 %make_values.1 = bf16[16,200,128]{2,1,0:T(8,128)(2,1)} custom-call(bf16[2,768,1024]{2,1,0:T(8,128)(2,1)S(1)} %bitcast.16, bf16[4,4,32,128]{3,2,1,0:T(8,128)(2,1)S(1)} %copy-done, bf16[4,4,224,128]{3,2,1,0:T(8,128)(2,1)S(1)} %collective-permute-done.2.late_ref, f32[768,512]{1,0:T(8,128)S(1)} %partial.3.begun_ref, ...), custom_call_target="tpu_custom_call" | custom-call | tf_op jit(solution)/shard_map/make_values/pallas_call | solution.py:328
  98.0 47.9 %all_to_all.26.rows_ref = bf16[16,200,128]{2,1,0:T(8,128)(2,1)S(1)} all-to-all(bf16[16,200,128]{2,1,0:T(8,128)(2,1)} %make_values.1), channel_id=1, replica_groups=mesh['y'=4,'x'=4,'z'=16,'c'=2] {'z'}, dimensions={0} | all-to-all | bytes 1638400 | tf_op jit(solution)/shard_map/all_to_all | solution.py:421
  145.9 6.7 %all-to-all-start.2 = ((bf16[16,192,128]{2,1,0:T(8,128)(2,1)}), bf16[16,192,128]{2,1,0:T(8,128)(2,1)S(1)}, u32[]{:S(2)}, u32[]{:S(2)}) async-start(bf16[16,192,128]{2,1,0:T(8,128)(2,1)} %get-tuple-element.15.key_ref), calls=%async_computation.2 | async-start | bytes 1572864 | tf_op jit(solution)/shard_map/all_to_all | solution.py:416
  152.6 0.6 join_first.1
  153.3 39.2 %all-to-all-done.2.rows_ref = bf16[16,192,128]{2,1,0:T(8,128)(2,1)S(1)} async-done(((bf16[16,192,128]{2,1,0:T(8,128)(2,1)}), bf16[16,192,128]{2,1,0:T(8,128)(2,1)S(1)}, u32[]{:S(2)}, u32[]{:S(2)}) %all-to-all-start.2) | async-done | bytes 786464 | tf_op jit(solution)/shard_map/all_to_all | solution.py:416
  192.5 4.9 %all-to-all-start.4 = ((f32[16,4,128]{2,1,0:T(4,128)}), f32[16,4,128]{2,1,0:T(4,128)S(1)}, u32[]{:S(2)}, u32[]{:S(2)}) async-start(f32[16,4,128]{2,1,0:T(4,128)} %join_first.1), calls=%async_computation.4 | async-start | bytes 65536 | tf_op jit(solution)/shard_map/all_to_all | solution.py:424
  197.4 0.9 store.1
  198.3 1.0 slice.4
  199.2 5.7 %all-to-all-done.4.rows_ref = f32[16,4,128]{2,1,0:T(4,128)S(1)} async-done(((f32[16,4,128]{2,1,0:T(4,128)}), f32[16,4,128]{2,1,0:T(4,128)S(1)}, u32[]{:S(2)}, u32[]{:S(2)}) %all-to-all-start.4) | async-done | bytes 32800 | tf_op jit(solution)/shard_map/all_to_all | solution.py:424
  (15 shorter events, 0.6 us)
Async XLA Ops:
  31.8 23.3 %all-to-all-start.1 = ((bf16[16,18,16,128]{3,2,1,0:T(8,128)(2,1)}), bf16[16,18,16,128]{3,2,1,0:T(8,128)(2,1)S(1)}, u32[]{:S(2)}, u32[]{:S(2)}) async-start(bf16[16,18,16,128]{3,2,1,0:T(8,128)(2,1)} %get-tuple-element.14), calls=%async_computation.1 | async-start | bytes 2359296 | tf_op jit(solution)/shard_map/all_to_all | solution.py:409
  38.8 43.0 %copy-start.1 = (bf16[8,1024]{1,0:T(8,128)(2,1)S(1)}, bf16[8,1024]{1,0:T(8,128)(2,1)}, u32[]{:S(2)}) copy-start(bf16[8,1024]{1,0:T(8,128)(2,1)} %query_ref.1) | copy-start | bytes 49156
  38.8 43.0 %copy-start.3 = (f32[128]{0:T(128)S(1)}, f32[128]{0:T(128)}, u32[]{:S(2)}) copy-start(f32[128]{0:T(128)} %param.14) | copy-start | bytes 1540
  43.4 38.4 %collective-permute-start = (bf16[4,96,2048]{2,1,0:T(8,128)(2,1)}, bf16[4,96,2048]{2,1,0:T(8,128)(2,1)S(1)}, u32[]{:S(2)}, u32[]{:S(2)}) collective-permute-start(bf16[4,96,2048]{2,1,0:T(8,128)(2,1)} %get-tuple-element.12), channel_id=1, source_target_pairs={{0,1},{1,0},{2,3},{3,2},{4,5},{5,4},{6,7},{7,6},{8,9},{9,8},{10,11... | collective-permute-start | bytes 4718600 | tf_op jit(solution)/shard_map/ppermute | solution.py:408
  55.1 33.6 %collective-permute-start.1 = (bf16[4,4,288,128]{3,2,1,0:T(8,128)(2,1)S(1)}, bf16[4,4,288,128]{3,2,1,0:T(8,128)(2,1)S(1)}, u32[]{:S(2)}, u32[]{:S(2)}) collective-permute-start(bf16[4,4,288,128]{3,2,1,0:T(8,128)(2,1)S(1)} %bitcast.17), channel_id=1, source_target_pairs={{0,1},{1,0},{2,3},{3,2},{4,5},{5,4},{6,7},{7,6},{8,9},{9,8},{10,11... | collective-permute-start | bytes 3538952 | tf_op jit(solution)/shard_map/ppermute | solution.py:413
  79.9 11.0 %collective-permute-start.2 = (bf16[4,4,224,128]{3,2,1,0:T(8,128)(2,1)S(1)}, bf16[4,4,224,128]{3,2,1,0:T(8,128)(2,1)S(1)}, u32[]{:S(2)}, u32[]{:S(2)}) collective-permute-start(bf16[4,4,224,128]{3,2,1,0:T(8,128)(2,1)S(1)} %bitcast.20), channel_id=1, source_target_pairs={{0,1},{1,0},{2,3},{3,2},{4,5},{5,4},{6,7},{7,6},{8,9},{9,8},{10,11... | collective-permute-start | bytes 2752520 | tf_op jit(solution)/shard_map/ppermute | solution.py:418
  87.7 1.0 copy-start.2
  88.7 2.2 %copy-start.4 = (f32[8]{0:T(128)S(1)}, f32[8]{0:T(128)}, u32[]{:S(2)}) copy-start(f32[8]{0:T(128)} %bias_ref.1) | copy-start | bytes 100
  90.9 0.9 copy-start
  145.9 46.6 %all-to-all-start.2 = ((bf16[16,192,128]{2,1,0:T(8,128)(2,1)}), bf16[16,192,128]{2,1,0:T(8,128)(2,1)S(1)}, u32[]{:S(2)}, u32[]{:S(2)}) async-start(bf16[16,192,128]{2,1,0:T(8,128)(2,1)} %get-tuple-element.15.key_ref), calls=%async_computation.2 | async-start | bytes 1572864 | tf_op jit(solution)/shard_map/all_to_all | solution.py:416
  192.5 12.5 %all-to-all-start.4 = ((f32[16,4,128]{2,1,0:T(4,128)}), f32[16,4,128]{2,1,0:T(4,128)S(1)}, u32[]{:S(2)}, u32[]{:S(2)}) async-start(f32[16,4,128]{2,1,0:T(4,128)} %join_first.1), calls=%async_computation.4 | async-start | bytes 65536 | tf_op jit(solution)/shard_map/all_to_all | solution.py:424

commit v4 on v3

--- a/solution.py
+++ b/solution.py
@@ -71,7 +71,7 @@
 
 def spread(pieces, count):
     zs, _, rows, width = pieces.shape
-    early = zs // 8
+    early = zs // 16
     return pl.pallas_call(
         spread_kernel,
         out_shape=(
@@ -334,22 +334,22 @@
     )(*on_chip(x), others[0], *on_chip(others[1], begun), keys, *on_chip(query), bias)
 
 
-def store_kernel(rows_ref, out_ref, sem):
-    copy = pltpu.make_async_copy(rows_ref, out_ref, sem)
-    copy.start()
-    copy.wait()
+def store_kernel(rows_ref, out_ref):
+    out_ref[...] = rows_ref[...]
 
 
 def store(rows):
+    blocks, span, hd = rows.shape
+    spec = pl.BlockSpec((blocks // 4, span, hd), lambda n: (n, 0, 0))
     return pl.pallas_call(
         store_kernel,
+        grid=(4,),
         out_shape=pltpu.HBM(rows.shape, rows.dtype),
-        in_specs=[pl.BlockSpec(memory_space=pl.ANY)],
-        out_specs=pl.BlockSpec(memory_space=pl.ANY),
-        scratch_shapes=[pltpu.SemaphoreType.DMA],
-        compiler_params=vmem(4),
+        in_specs=[spec],
+        out_specs=spec,
+        compiler_params=vmem(8),
         name="store",
-    )(rows)
+    )(*off_chip(rows))
 
 
 def join_first_kernel(rows_ref, out_ref):

time: 206 us -> 206 us (level)
  waiting for transfers between devices: 54.7 us -> 51.5 us
  Pallas kernels: 23.1 us -> 25.4 us
    all_to_all x1, waiting for transfers between devices: 5.74 us -> 3.37 us  [shards(): everything = lax.all_to_all(joined, SP, 0, 0, tiled=True)]
    pallas_call x1, Pallas kernels: 0.89 us -> 3.26 us  [store(): pl.pallas_call(store_kernel, grid=(4,), out_shape=pltpu.HBM(rows.shape, r...]
  transfers between devices with their start and end apart: 6 -> 6, of which waited for: 3 -> 3; matrix products, arithmetic and copies ran while one was open for 0% -> 0% of each run, Pallas kernels for 7% -> 9%
where the time goes in v4:
time: 206 us; the launch traced here: 205 us
  blocking collectives  100 us (49%)
  waiting for transfers between devices  51.5 us (25%)
  Pallas kernels  25.4 us (12%)
  starting transfers between devices  24 us (12%)
  local copies, waits for them, and re-layouts  2.56 us (1%)
    all_to_all x1, blocking collectives, shards(): got_values = lax.all_to_all(values, 'z', 0, 0, tiled=True)  48 us
    all_to_all x1, waiting for transfers between devices, shards(): got_keys = lax.all_to_all(keys, 'z', 0, 0, tiled=True)  39.2 us
    all_to_all x1, blocking collectives, to_all(): lax.all_to_all(jnp.broadcast_to(piece[None], (count, *piece.shape)), axis...  29.2 us
    all_gather x1, blocking collectives, shards(): late = lax.all_gather(late, SP).reshape(ys, xs, -1, head_dim)  23.2 us
    all_to_all x1, waiting for transfers between devices, shards(): early = lax.all_to_all(early, SP, 0, 0, tiled=True)  8.94 us
    all_to_all x1, starting transfers between devices, shards(): early = lax.all_to_all(early, SP, 0, 0, tiled=True)  7.03 us
    all_to_all x1, starting transfers between devices, shards(): got_keys = lax.all_to_all(keys, 'z', 0, 0, tiled=True)  6.68 us
    pallas_call x1, Pallas kernels, make_values(): pl.pallas_call(values_kernel, out_shape=pltpu.HBM((blocks, span + EXTRA,...  6.18 us
  transfers between devices with their start and end apart: 6, of which 3 were waited for; matrix products, arithmetic and copies ran while one was open for 0% of the time, Pallas kernels for 9%

profile of v4, /device:TPU:32, one launch (start us, length us, event | category | flops | bytes accessed | tf_op | source)
XLA Modules:
  0.0 204.8 jit_solution(18310497511994609560)
XLA Ops:
  0.6 0.7 dynamic-slice_bitcast_fusion
  1.4 29.2 %all_to_all.25.pieces_ref = bf16[16,2,16,128]{3,2,1,0:T(8,128)(2,1)S(1)} all-to-all(bf16[16,2,16,128]{3,2,1,0:T(8,128)(2,1)S(1)} %broadcast_in_dim.2), channel_id=1, replica_groups=mesh['y'=4,'x'=4,'z'=16,'c'=2] {'z'}, dimensions={0} | all-to-all | bytes 262144 | tf_op jit(solution)/shard_map/all_to_all | solution.py:25
  30.6 1.1 spread.1
  31.7 7.0 %all-to-all-start.1 = ((bf16[16,17,16,128]{3,2,1,0:T(8,128)(2,1)}), bf16[16,17,16,128]{3,2,1,0:T(8,128)(2,1)S(1)}, u32[]{:S(2)}, u32[]{:S(2)}) async-start(bf16[16,17,16,128]{3,2,1,0:T(8,128)(2,1)} %get-tuple-element.14), calls=%async_computation.1 | async-start | bytes 2228224 | tf_op jit(solution)/shard_map/all_to_all | solution.py:409
  38.8 4.6 %norm_halves.1 = (bf16[4,96,2048]{2,1,0:T(8,128)(2,1)}, bf16[4,96,2048]{2,1,0:T(8,128)(2,1)}) custom-call(bf16[8,96,2048]{2,1,0:T(8,128)(2,1)} %tokens_ref.1, f32[1,2048]{1,0:T(1,128)} %bitcast.26), custom_call_target="tpu_custom_call" | custom-call | tf_op jit(solution)/shard_map/norm_halves/pallas_call | solution.py:49
  43.4 1.9 collective-permute-start
  45.3 8.9 %all-to-all-done.1 = bf16[16,17,16,128]{3,2,1,0:T(8,128)(2,1)S(1)} async-done(((bf16[16,17,16,128]{3,2,1,0:T(8,128)(2,1)}), bf16[16,17,16,128]{3,2,1,0:T(8,128)(2,1)S(1)}, u32[]{:S(2)}, u32[]{:S(2)}) %all-to-all-start.1) | async-done | bytes 1114144 | tf_op jit(solution)/shard_map/all_to_all | solution.py:409
  54.3 1.9 collective-permute-start.1
  56.2 23.2 %all-gather = bf16[240,16,128]{2,1,0:T(8,128)(2,1)S(1)} all-gather(bf16[15,16,128]{2,1,0:T(8,128)(2,1)S(1)} %get-tuple-element.17), channel_id=2, replica_groups=mesh['y'=4,'x'=4,'z'=16,'c'=2] {'y','x'}, dimensions={0}, use_global_device_ids=true | all-gather | bytes 1044480 | tf_op jit(solution)/shard_map/all_gather | solution.py:417
  79.4 1.9 collective-permute-start.2
  81.4 4.9 %arrange.1 = (bf16[2,2,384,1024]{3,2,1,0:T(8,128)(2,1)S(1)}, bf16[4,8,512]{2,1,0:T(8,128)(2,1)S(1)}) custom-call(bf16[4,96,2048]{2,1,0:T(8,128)(2,1)} %get-tuple-element.11.kept_hbm, bf16[4,96,2048]{2,1,0:T(8,128)(2,1)S(1)} %collective-permute-done.came_hbm, bf16[8,1024]{1,0:T(8,128)(2,1)S(1)} %copy-done.1, f32[1,128]{1,0:T(1,128)S(1)} %bitcast.23), custom_call_target="tpu_custom_call" | custom-call | tf_op jit(solution)/shard_map/arrange/pallas_call | solution.py:159
  86.3 1.0 partial.2.begun_ref
  87.2 1.0 partial.3.begun_ref
  88.3 2.2 %make_keys.1 = (bf16[16,192,128]{2,1,0:T(8,128)(2,1)}, bf16[4,4,16,128]{3,2,1,0:T(8,128)(2,1)}) custom-call(bf16[2,768,1024]{2,1,0:T(8,128)(2,1)S(1)} %bitcast.15, bf16[4,4,272,128]{3,2,1,0:T(8,128)(2,1)S(1)} %collective-permute-done.1.rows_ref, f32[768,512]{1,0:T(8,128)S(1)} %partial.2.begun_ref, f32[1,128]{1,0:T(1,128)S(1)} %bitcast.22), custom_call_target="tpu_custom_call" | custom-call | tf_op jit(solution)/shard_map/make_keys/pallas_call | solution.py:241
  90.5 0.8 copy-done
  91.3 6.2 %make_values.1 = bf16[16,200,128]{2,1,0:T(8,128)(2,1)} custom-call(bf16[2,768,1024]{2,1,0:T(8,128)(2,1)S(1)} %bitcast.16, bf16[4,4,16,128]{3,2,1,0:T(8,128)(2,1)S(1)} %copy-done, bf16[4,4,240,128]{3,2,1,0:T(8,128)(2,1)S(1)} %collective-permute-done.2.late_ref, f32[768,512]{1,0:T(8,128)S(1)} %partial.3.begun_ref, ...), custom_call_target="tpu_custom_call" | custom-call | tf_op jit(solution)/shard_map/make_values/pallas_call | solution.py:328
  97.5 48.0 %all_to_all.26.rows_ref = bf16[16,200,128]{2,1,0:T(8,128)(2,1)S(1)} all-to-all(bf16[16,200,128]{2,1,0:T(8,128)(2,1)} %make_values.1), channel_id=1, replica_groups=mesh['y'=4,'x'=4,'z'=16,'c'=2] {'z'}, dimensions={0} | all-to-all | bytes 1638400 | tf_op jit(solution)/shard_map/all_to_all | solution.py:421
  145.5 6.7 %all-to-all-start.2 = ((bf16[16,192,128]{2,1,0:T(8,128)(2,1)}), bf16[16,192,128]{2,1,0:T(8,128)(2,1)S(1)}, u32[]{:S(2)}, u32[]{:S(2)}) async-start(bf16[16,192,128]{2,1,0:T(8,128)(2,1)} %get-tuple-element.15.key_ref), calls=%async_computation.2 | async-start | bytes 1572864 | tf_op jit(solution)/shard_map/all_to_all | solution.py:416
  152.2 0.6 join_first.1
  152.8 39.2 %all-to-all-done.2.rows_ref = bf16[16,192,128]{2,1,0:T(8,128)(2,1)S(1)} async-done(((bf16[16,192,128]{2,1,0:T(8,128)(2,1)}), bf16[16,192,128]{2,1,0:T(8,128)(2,1)S(1)}, u32[]{:S(2)}, u32[]{:S(2)}) %all-to-all-start.2) | async-done | bytes 786464 | tf_op jit(solution)/shard_map/all_to_all | solution.py:416
  192.0 4.6 %all-to-all-start.4 = ((f32[16,4,128]{2,1,0:T(4,128)}), f32[16,4,128]{2,1,0:T(4,128)S(1)}, u32[]{:S(2)}, u32[]{:S(2)}) async-start(f32[16,4,128]{2,1,0:T(4,128)} %join_first.1), calls=%async_computation.4 | async-start | bytes 65536 | tf_op jit(solution)/shard_map/all_to_all | solution.py:424
  196.6 3.3 %store.1 = bf16[16,192,128]{2,1,0:T(8,128)(2,1)} custom-call(bf16[16,192,128]{2,1,0:T(8,128)(2,1)} %copy-done.5), custom_call_target="tpu_custom_call" | custom-call | tf_op jit(solution)/shard_map/store/pallas_call | solution.py:344
  199.9 1.0 slice.4
  200.8 3.4 %all-to-all-done.4.rows_ref = f32[16,4,128]{2,1,0:T(4,128)S(1)} async-done(((f32[16,4,128]{2,1,0:T(4,128)}), f32[16,4,128]{2,1,0:T(4,128)S(1)}, u32[]{:S(2)}, u32[]{:S(2)}) %all-to-all-start.4) | async-done | bytes 32800 | tf_op jit(solution)/shard_map/all_to_all | solution.py:424
  (17 shorter events, 0.7 us)
Async XLA Ops:
  31.7 22.5 %all-to-all-start.1 = ((bf16[16,17,16,128]{3,2,1,0:T(8,128)(2,1)}), bf16[16,17,16,128]{3,2,1,0:T(8,128)(2,1)S(1)}, u32[]{:S(2)}, u32[]{:S(2)}) async-start(bf16[16,17,16,128]{3,2,1,0:T(8,128)(2,1)} %get-tuple-element.14), calls=%async_computation.1 | async-start | bytes 2228224 | tf_op jit(solution)/shard_map/all_to_all | solution.py:409
  38.8 42.6 %copy-start.1 = (bf16[8,1024]{1,0:T(8,128)(2,1)S(1)}, bf16[8,1024]{1,0:T(8,128)(2,1)}, u32[]{:S(2)}) copy-start(bf16[8,1024]{1,0:T(8,128)(2,1)} %query_ref.1) | copy-start | bytes 49156
  38.8 42.6 %copy-start.3 = (f32[128]{0:T(128)S(1)}, f32[128]{0:T(128)}, u32[]{:S(2)}) copy-start(f32[128]{0:T(128)} %param.14) | copy-start | bytes 1540
  43.4 37.9 %collective-permute-start = (bf16[4,96,2048]{2,1,0:T(8,128)(2,1)}, bf16[4,96,2048]{2,1,0:T(8,128)(2,1)S(1)}, u32[]{:S(2)}, u32[]{:S(2)}) collective-permute-start(bf16[4,96,2048]{2,1,0:T(8,128)(2,1)} %get-tuple-element.12), channel_id=1, source_target_pairs={{0,1},{1,0},{2,3},{3,2},{4,5},{5,4},{6,7},{7,6},{8,9},{9,8},{10,11... | collective-permute-start | bytes 4718600 | tf_op jit(solution)/shard_map/ppermute | solution.py:408
  54.3 34.0 %collective-permute-start.1 = (bf16[4,4,272,128]{3,2,1,0:T(8,128)(2,1)S(1)}, bf16[4,4,272,128]{3,2,1,0:T(8,128)(2,1)S(1)}, u32[]{:S(2)}, u32[]{:S(2)}) collective-permute-start(bf16[4,4,272,128]{3,2,1,0:T(8,128)(2,1)S(1)} %bitcast.17), channel_id=1, source_target_pairs={{0,1},{1,0},{2,3},{3,2},{4,5},{5,4},{6,7},{7,6},{8,9},{9,8},{10,11... | collective-permute-start | bytes 3342344 | tf_op jit(solution)/shard_map/ppermute | solution.py:413
  79.4 11.0 %collective-permute-start.2 = (bf16[4,4,240,128]{3,2,1,0:T(8,128)(2,1)S(1)}, bf16[4,4,240,128]{3,2,1,0:T(8,128)(2,1)S(1)}, u32[]{:S(2)}, u32[]{:S(2)}) collective-permute-start(bf16[4,4,240,128]{3,2,1,0:T(8,128)(2,1)S(1)} %bitcast.20), channel_id=1, source_target_pairs={{0,1},{1,0},{2,3},{3,2},{4,5},{5,4},{6,7},{7,6},{8,9},{9,8},{10,11... | collective-permute-start | bytes 2949128 | tf_op jit(solution)/shard_map/ppermute | solution.py:418
  87.2 1.0 copy-start.2
  88.3 2.2 %copy-start.4 = (f32[8]{0:T(128)S(1)}, f32[8]{0:T(128)}, u32[]{:S(2)}) copy-start(f32[8]{0:T(128)} %bias_ref.1) | copy-start | bytes 100
  90.5 0.8 copy-start
  145.5 46.5 %all-to-all-start.2 = ((bf16[16,192,128]{2,1,0:T(8,128)(2,1)}), bf16[16,192,128]{2,1,0:T(8,128)(2,1)S(1)}, u32[]{:S(2)}, u32[]{:S(2)}) async-start(bf16[16,192,128]{2,1,0:T(8,128)(2,1)} %get-tuple-element.15.key_ref), calls=%async_computation.2 | async-start | bytes 1572864 | tf_op jit(solution)/shard_map/all_to_all | solution.py:416
  192.0 4.6 %copy-start.5 = (bf16[16,192,128]{2,1,0:T(8,128)(2,1)}, bf16[16,192,128]{2,1,0:T(8,128)(2,1)S(1)}, u32[]{:S(2)}) copy-start(bf16[16,192,128]{2,1,0:T(8,128)(2,1)S(1)} %all-to-all-done.2.rows_ref) | copy-start | bytes 2359300
  192.0 12.2 %all-to-all-start.4 = ((f32[16,4,128]{2,1,0:T(4,128)}), f32[16,4,128]{2,1,0:T(4,128)S(1)}, u32[]{:S(2)}, u32[]{:S(2)}) async-start(f32[16,4,128]{2,1,0:T(4,128)} %join_first.1), calls=%async_computation.4 | async-start | bytes 65536 | tf_op jit(solution)/shard_map/all_to_all | solution.py:424

commit v5 on v4

--- a/solution.py
+++ b/solution.py
@@ -35,48 +35,74 @@
     return to_all(jnp.stack(parts), "z")
 
 
-def norm_kernel(tokens_ref, gain_ref, kept_ref, sent_ref):
+def norm_kernel(tokens_ref, gain_ref, w_key_ref, w_value_ref, kept_ref, sent_ref):
     core = lax.axis_index("c")
+    step = pl.program_id(0)
     gain = gain_ref[...]
+    length = kept_ref.shape[1]
+    extra = sent_ref.shape[1] - length
     kept_ref[0] = root_norm(tokens_ref[core].astype(F32), gain).astype(BF16)
-    sent_ref[0] = root_norm(tokens_ref[1 - core].astype(F32), gain).astype(BF16)
-
-
-def norm_halves(tokens, in_gain):
+    sent_ref[0, :length] = root_norm(tokens_ref[1 - core].astype(F32), gain).astype(BF16)
+    width = w_key_ref.shape[1]
+    across = sent_ref.shape[2] // width
+    half = pl.num_programs(0) // 2
+    at = pl.multiple_of(lax.rem(step, half) * (extra * across), 32)
+    rows = jnp.where(
+        step < half,
+        w_key_ref[pl.ds(at, extra * across), :],
+        w_value_ref[pl.ds(at, extra * across), :],
+    )
+    for m in range(across):
+        sent_ref[0, length:, m * width : (m + 1) * width] = rows[m * extra : (m + 1) * extra]
+
+
+def norm_halves(tokens, in_gain, w_key, w_value):
     seq_count, length, model = tokens.shape
-    half = pltpu.HBM((seq_count // 2, length, model), BF16)
-    block = pl.BlockSpec((1, length, model), lambda i: (i, 0, 0))
+    seqs = seq_count // 2
+    extra = 2 * w_key.size // (seqs * model)
+    whole = pl.BlockSpec(w_key.shape, lambda i: (0, 0))
     return pl.pallas_call(
         norm_kernel,
-        grid=(seq_count // 2,),
-        out_shape=(half, half),
+        grid=(seqs,),
+        out_shape=(
+            pltpu.HBM((seqs, length, model), BF16),
+            pltpu.HBM((seqs, length + extra, model), BF16),
+        ),
         in_specs=[
             pl.BlockSpec((2, length, model), lambda i: (i, 0, 0)),
             pl.BlockSpec((1, model), lambda i: (0, 0)),
+            whole,
+            whole,
         ],
-        out_specs=(block, block),
+        out_specs=(
+            pl.BlockSpec((1, length, model), lambda i: (i, 0, 0)),
+            pl.BlockSpec((1, length + extra, model), lambda i: (i, 0, 0)),
+        ),
         compiler_params=vmem(16),
         name="norm_halves",
-    )(*off_chip(tokens, in_gain.reshape(1, model)))
+    )(*off_chip(tokens, in_gain.reshape(1, model), w_key, w_value))
+
+
+def from_here(distance):
+    return lax.rem(lax.axis_index("z") + distance, lax.axis_size("z"))
 
 
 def spread_kernel(pieces_ref, early_ref, late_ref):
-    zs = pieces_ref.shape[0]
-    early = early_ref.shape[1] - zs
-    for n in range(early_ref.shape[0]):
-        early_ref[n, :zs] = pieces_ref[:, 0]
-        early_ref[n, zs:] = pieces_ref[:early, 1]
-    late_ref[...] = pieces_ref[early:, 1]
+    for k in range(late_ref.shape[0]):
+        at = from_here(k + 1)
+        piece = pieces_ref[at, 0]
+        for n in range(early_ref.shape[0]):
+            early_ref[n, k] = piece
+        late_ref[k] = pieces_ref[at, 1]
 
 
 def spread(pieces, count):
     zs, _, rows, width = pieces.shape
-    early = zs // 16
     return pl.pallas_call(
         spread_kernel,
         out_shape=(
-            jax.ShapeDtypeStruct((count, zs + early, rows, width), pieces.dtype),
-            jax.ShapeDtypeStruct((zs - early, rows, width), pieces.dtype),
+            jax.ShapeDtypeStruct((count, zs - 1, rows, width), pieces.dtype),
+            jax.ShapeDtypeStruct((zs - 1, rows, width), pieces.dtype),
         ),
         compiler_params=vmem(8),
         name="spread",
@@ -100,30 +126,45 @@
     return high, (values - high.astype(F32)).astype(BF16)
 
 
-def arrange_kernel(
-    kept_hbm, came_hbm, query_ref, gain_ref, x_ref, grouped_ref, kept_ref, came_ref, sems
-):
-    core = lax.axis_index("c")
-    loads = [
-        pltpu.make_async_copy(kept_hbm, kept_ref, sems.at[0]),
-        pltpu.make_async_copy(came_hbm, came_ref, sems.at[1]),
-    ]
-    for load in loads:
-        load.start()
-    seqs, length, model = kept_ref.shape
-    hd = gain_ref.shape[1]
-    heads = query_ref.shape[1] // hd
-    kv_heads = grouped_ref.shape[2] // hd
+def arranged(tokens_ref, x_ref):
+    half, _, model_half = x_ref.shape
+    model = half * model_half
     zs, xs = lax.axis_size("z"), lax.axis_size("x")
     held = model // zs // 2
     rows = held // xs
+    hd = 128
     part = hd // rows
     deep = part * 2 * held
     source = lax.broadcasted_iota(jnp.int32, (deep, 2 * hd), 0)
     column = lax.broadcasted_iota(jnp.int32, (deep, 2 * hd), 1)
     inside = column % hd
     offset = source - (inside // rows) * (2 * held) - inside % rows - (column // hd) * rows
-
+    seqs = tokens_ref.shape[0]
+    length = x_ref.shape[1] // seqs
+    groups = []
+    for n in range(zs // part):
+        columns = [
+            tokens_ref[:, :length, pl.ds(pl.multiple_of(from_here(n * part + k) * hd, hd), hd)]
+            for k in range(part)
+        ]
+        groups.append(
+            jnp.concatenate([c.reshape(seqs * length, hd) for c in columns], axis=1)
+        )
+    for h in range(half):
+        for r in range(0, xs, 2):
+            pick = (offset == h * held + r * rows).astype(BF16)
+            for n in range(zs // part):
+                moved = jnp.dot(groups[n], pick, preferred_element_type=F32).astype(BF16)
+                for k in range(2):
+                    start = (r + k) * zs * rows + n * hd
+                    x_ref[h, :, start : start + hd] = moved[:, k * hd : (k + 1) * hd]
+
+
+def group_queries(query_ref, gain_ref, grouped_ref):
+    core = lax.axis_index("c")
+    hd = gain_ref.shape[1]
+    seqs, heads, width = grouped_ref.shape
+    kv_heads = width // hd
     query = query_ref[...].astype(F32)
     row = lax.broadcasted_iota(jnp.int32, (heads, hd), 0)
     per_group = heads // kv_heads
@@ -135,129 +176,141 @@
                 head = root_norm(mine[:, j * hd : (j + 1) * hd], gain_ref[...])
                 block = jnp.where(row == j, head, block)
             grouped_ref[i, :, g * hd : (g + 1) * hd] = block.astype(BF16)
-    for load in loads:
-        load.wait()
-    kept = kept_ref[...].reshape(seqs * length, model)
-    came = came_ref[...].reshape(seqs * length, model)
-    for half in range(2):
-        for r in range(0, xs, 2):
-            pick = (offset == half * held + r * rows).astype(BF16)
-            for n in range(zs // part):
-                for values, at in ((kept, core), (came, 1 - core)):
-                    moved = jnp.dot(
-                        values[:, n * deep : (n + 1) * deep], pick, preferred_element_type=F32
-                    ).astype(BF16)
-                    for k in range(2):
-                        start = (r + k) * zs * rows + n * hd
-                        x_ref[half, at, :, start : start + hd] = moved[:, k * hd : (k + 1) * hd]
-
-
-def arrange(kept, came, new_query, q_gain, kv_heads):
+
+
+def arrange_kept_kernel(kept_hbm, query_ref, gain_ref, x_ref, grouped_ref, kept_ref, sem):
+    load = pltpu.make_async_copy(kept_hbm, kept_ref, sem)
+    load.start()
+    group_queries(query_ref, gain_ref, grouped_ref)
+    load.wait()
+    arranged(kept_ref, x_ref)
+
+
+def arrange_came_kernel(came_ref, x_ref, shards_ref):
+    arranged(came_ref, x_ref)
+    seqs, rows, model = came_ref.shape
+    length = x_ref.shape[1] // seqs
+    extra = rows - length
+    _, held, width = shards_ref.shape
+    for i in range(seqs):
+        for m in range(model // width):
+            which, at = divmod((i * (model // width) + m) * extra, held)
+            shards_ref[which, at : at + extra] = came_ref[
+                i, length:, m * width : (m + 1) * width
+            ]
+
+
+def arrange_kept(kept, new_query, q_gain, kv_heads):
     seqs, length, model = kept.shape
     hd = q_gain.shape[0]
     heads = new_query.shape[1] // hd
     return pl.pallas_call(
-        arrange_kernel,
+        arrange_kept_kernel,
         out_shape=(
-            pltpu.VMEM((2, 2, seqs * length, model // 2), BF16),
+            pltpu.VMEM((2, seqs * length, model // 2), BF16),
             pltpu.VMEM((seqs, heads, kv_heads * hd), BF16),
         ),
-        in_specs=[pl.BlockSpec(memory_space=pl.ANY)] * 2
+        in_specs=[pl.BlockSpec(memory_space=pl.ANY)]
         + [pl.BlockSpec(memory_space=pltpu.VMEM)] * 2,
-        scratch_shapes=[
-            pltpu.VMEM(kept.shape, BF16),
-            pltpu.VMEM(kept.shape, BF16),
-            pltpu.SemaphoreType.DMA((2,)),
-        ],
-        compiler_params=vmem(32),
-        name="arrange",
-    )(*off_chip(kept), came, new_query, q_gain.reshape(1, hd))
-
-
-def two_heads(refs, head):
+        scratch_shapes=[pltpu.VMEM(kept.shape, BF16), pltpu.SemaphoreType.DMA],
+        compiler_params=vmem(20),
+        name="arrange_kept",
+    )(*off_chip(kept), new_query, q_gain.reshape(1, hd))
+
+
+def arrange_came(came, length, shard):
+    seqs, _, model = came.shape
+    return pl.pallas_call(
+        arrange_came_kernel,
+        out_shape=(
+            pltpu.VMEM((2, seqs * length, model // 2), BF16),
+            pltpu.VMEM((2, *shard), BF16),
+        ),
+        compiler_params=vmem(20),
+        name="arrange_came",
+    )(came)
+
+
+def both(refs, core):
+    return jnp.concatenate([ref[core] for ref in refs], axis=0)
+
+
+def two_heads(shard, rows_ref, head):
+    parts, hd = rows_ref.shape[1], rows_ref.shape[3]
+    rows = shard.shape[0] // parts
     columns = []
     for g in (head, head + 1):
-        blocks = [ref[g, n, first:last] for n in range(refs[0][0].shape[1]) for ref, first, last in refs]
+        blocks = []
+        for n in range(parts):
+            blocks.append(shard[n * rows : (n + 1) * rows, g * hd : (g + 1) * hd])
+            blocks.append(rows_ref[g, n])
         columns.append(jnp.concatenate(blocks, axis=0))
     return jnp.concatenate(columns, axis=1)
 
 
-def key_part(early_ref, held):
-    return ((early_ref, 0, held),)
-
-
-def value_parts(early_ref, late_ref, held):
-    first = held if early_ref.shape[2] > held else 0
-    return ((early_ref, first, early_ref.shape[2]), (late_ref, 0, late_ref.shape[2]))
-
-
-def partial_kernel(*refs):
-    x_ref, *rows_refs, out_ref = refs
-    x = x_ref[lax.axis_index("c")]
-    heads, count, _, hd = rows_refs[0].shape
-    held = x.shape[1] // count
-    parts = key_part(*rows_refs, held) if len(rows_refs) == 1 else value_parts(*rows_refs, held)
+def partial_kernel(kept_ref, came_ref, shard_ref, rows_ref, out_ref):
+    x = both((kept_ref, came_ref), lax.axis_index("c"))
+    heads, _, _, hd = rows_ref.shape
+    shard = shard_ref[...]
     for g in range(0, heads, 2):
         out_ref[:, g * hd : (g + 2) * hd] = jnp.dot(
-            x, two_heads(parts, g), preferred_element_type=F32
+            x, two_heads(shard, rows_ref, g), preferred_element_type=F32
         )
 
 
-def partial_product(x, rows):
-    width = rows[0].shape[0] * rows[0].shape[-1]
+def partial_product(x, shard, rows):
     return pl.pallas_call(
         partial_kernel,
-        out_shape=pltpu.VMEM((x.shape[1], width), F32),
+        out_shape=pltpu.VMEM((2 * x[0].shape[1], shard.shape[1]), F32),
         compiler_params=vmem(16),
         name="partial",
-    )(*on_chip(x), *rows)
+    )(*on_chip(*x), shard, rows)
 
 
 def place(ref, seqs, length, g, head):
+    core = lax.axis_index("c")
     for n in range(2 * seqs):
-        h, i = divmod(n, seqs)
-        ref[g * seqs + i, h * length : (h + 1) * length, :] = head[n * length : (n + 1) * length]
-
-
-def keys_kernel(x_ref, rows_ref, begun_ref, gain_ref, key_ref, rest_ref):
-    x = x_ref[1 - lax.axis_index("c")]
+        half, i = divmod(n, seqs)
+        at = pl.multiple_of((core if half == 0 else 1 - core) * length, 32)
+        ref[g * seqs + i, pl.ds(at, length), :] = head[n * length : (n + 1) * length]
+
+
+def keys_kernel(kept_ref, came_ref, shards_ref, rows_ref, begun_ref, gain_ref, key_ref):
+    x = both((kept_ref, came_ref), 1 - lax.axis_index("c"))
     gain = gain_ref[...]
+    shard = shards_ref[0]
     kv_heads, hd = rows_ref.shape[0], gain.shape[1]
-    held = x.shape[1] // rows_ref.shape[1]
     seqs = key_ref.shape[0] // kv_heads
     for g in range(0, kv_heads, 2):
         raw = begun_ref[:, g * hd : (g + 2) * hd] + jnp.dot(
-            x, two_heads(key_part(rows_ref, held), g), preferred_element_type=F32
+            x, two_heads(shard, rows_ref, g), preferred_element_type=F32
         )
         for k in range(2):
             head = root_norm(raw[:, k * hd : (k + 1) * hd], gain).astype(BF16)
             place(key_ref, seqs, key_ref.shape[1] // 2, g + k, head)
-    rest_ref[...] = rows_ref[:, :, held:]
-
-
-def make_keys(x, other, begun, gain, seqs):
-    kv_heads, parts, rows, hd = other.shape
-    rest = rows - x.shape[2] // parts
+
+
+def make_keys(x, shards_other, other, begun, gain, seqs):
+    kv_heads, hd = other.shape[0], other.shape[3]
     return pl.pallas_call(
         keys_kernel,
-        out_shape=(
-            pltpu.HBM((kv_heads * seqs, x.shape[1] // seqs, hd), BF16),
-            pltpu.HBM((kv_heads, parts, rest, hd), BF16),
-        ),
+        out_shape=pltpu.HBM((kv_heads * seqs, 2 * x[0].shape[1] // seqs, hd), BF16),
         compiler_params=vmem(16),
         name="make_keys",
-    )(*on_chip(x, other, begun), gain.reshape(1, hd))
-
-
-def values_kernel(x_ref, early_ref, late_ref, begun_ref, key_ref, query_ref, bias_ref, value_ref):
+    )(*on_chip(*x), shards_other, *on_chip(other, begun), gain.reshape(1, hd))
+
+
+def values_kernel(
+    kept_ref, came_ref, shards_ref, rows_ref, begun_ref, key_ref, query_ref, bias_ref, value_ref
+):
     core = lax.axis_index("c")
     seqs, heads, width = query_ref.shape
     hd = key_ref.shape[2]
     span = key_ref.shape[1]
     kv_heads = width // hd
     per_group = heads // kv_heads
-    x = x_ref[1 - core]
-    held = x.shape[1] // early_ref.shape[1]
+    x = both((kept_ref, came_ref), 1 - core)
+    shard = shards_ref[1]
 
     row = lax.broadcasted_iota(jnp.int32, (heads, 1), 0)
     bias = jnp.zeros((heads, 1), F32)
@@ -290,7 +343,7 @@
 
     for g in range(0, kv_heads, 2):
         raw = begun_ref[:, g * hd : (g + 2) * hd] + jnp.dot(
-            x, two_heads(value_parts(early_ref, late_ref, held), g), preferred_element_type=F32
+            x, two_heads(shard, rows_ref, g), preferred_element_type=F32
         )
         for k in range(2):
             place(value_ref, seqs, span // 2, g + k, raw[:, k * hd : (k + 1) * hd].astype(BF16))
@@ -322,16 +375,16 @@
             ).astype(BF16)
 
 
-def make_values(x, others, begun, keys, query, bias):
+def make_values(x, shards_other, other, begun, keys, query, bias):
     blocks, span, hd = keys.shape
     here = pl.BlockSpec(memory_space=pltpu.VMEM)
     return pl.pallas_call(
         values_kernel,
         out_shape=pltpu.HBM((blocks, span + EXTRA, hd), BF16),
-        in_specs=[here] * 6 + [pl.BlockSpec(memory_space=pltpu.SMEM)],
+        in_specs=[here] * 7 + [pl.BlockSpec(memory_space=pltpu.SMEM)],
         compiler_params=vmem(24),
         name="make_values",
-    )(*on_chip(x), others[0], *on_chip(others[1], begun), keys, *on_chip(query), bias)
+    )(*on_chip(*x), shards_other, *on_chip(other, begun), keys, *on_chip(query), bias)
 
 
 def store_kernel(rows_ref, out_ref):
@@ -394,7 +447,7 @@
 
 
 def shards(tokens, in_gain, w_key, w_value, k_gain, new_query, q_gain, stick_bias):
-    seq_count, tok_seq, model_width = tokens.shape
+    seq_count, tok_seq, _ = tokens.shape
     head_dim = k_gain.shape[0]
     heads = stick_bias.shape[0]
     kv_heads = w_key.shape[1] // head_dim
@@ -403,21 +456,22 @@
     trade = functools.partial(lax.ppermute, axis_name="c", perm=[(0, 1), (1, 0)])
     ys, xs = lax.axis_size("y"), lax.axis_size("x")
     pieces = along_z(w_key, w_value)
-    kept, sent = norm_halves(tokens, in_gain)
+    kept, sent = norm_halves(tokens, in_gain, w_key, w_value)
     early, late = spread(pieces, ys * xs)
     came = trade(sent)
     early = lax.all_to_all(early, SP, 0, 0, tiled=True)
-    x, query = arrange(kept, came, new_query, q_gain, kv_heads)
-    x = x.reshape(2, seq_count * tok_seq, model_width // 2)
+    x_kept, query = arrange_kept(kept, new_query, q_gain, kv_heads)
+    x_came, shards_other = arrange_came(came, tok_seq, w_key.shape)
+    x = (x_kept, x_came)
     early = early.reshape(ys, xs, -1, head_dim)
     early_other = trade(early)
-    begun = partial_product(x, (early,))
-    keys, early_other = make_keys(x, early_other, begun, k_gain, seqs)
+    begun = partial_product(x, w_key, early)
+    keys = make_keys(x, shards_other, early_other, begun, k_gain, seqs)
     got_keys = lax.all_to_all(keys, "z", 0, 0, tiled=True)
     late = lax.all_gather(late, SP).reshape(ys, xs, -1, head_dim)
     late_other = trade(late)
-    begun = partial_product(x, (early, late))
-    values = make_values(x, (early_other, late_other), begun, keys, query, stick_bias)
+    begun = partial_product(x, w_value, late)
+    values = make_values(x, shards_other, late_other, begun, keys, query, stick_bias)
     got_values = lax.all_to_all(values, "z", 0, 0, tiled=True)
     stored = store(got_keys)
     joined = join_first(got_values, ys * xs)

time: 206 us -> 204 us (level)
    pallas_call x5 -> x6, Pallas kernels: 13.6 us -> 14.1 us  [the longest x1 4.62 us: norm_halves(): pl.pallas_call(norm_kernel, grid=(seqs,), out_shape=(pltpu.HBM((seqs, len...]
where the time goes in v5:
time: 204 us; the launch traced here: 203 us
  blocking collectives  101 us (50%)
  waiting for transfers between devices  49.9 us (24%)
  Pallas kernels  25.8 us (13%)
  starting transfers between devices  23.9 us (12%)
    all_to_all x1, blocking collectives, shards(): got_values = lax.all_to_all(values, 'z', 0, 0, tiled=True)  48.1 us
    all_to_all x1, waiting for transfers between devices, shards(): got_keys = lax.all_to_all(keys, 'z', 0, 0, tiled=True)  39.2 us
    all_to_all x1, blocking collectives, to_all(): lax.all_to_all(jnp.broadcast_to(piece[None], (count, *piece.shape)), axis...  29.2 us
    all_gather x1, blocking collectives, shards(): late = lax.all_gather(late, SP).reshape(ys, xs, -1, head_dim)  23.3 us
    all_to_all x1, waiting for transfers between devices, shards(): early = lax.all_to_all(early, SP, 0, 0, tiled=True)  7.35 us
    all_to_all x1, starting transfers between devices, shards(): early = lax.all_to_all(early, SP, 0, 0, tiled=True)  7.03 us
    all_to_all x1, starting transfers between devices, shards(): got_keys = lax.all_to_all(keys, 'z', 0, 0, tiled=True)  6.72 us
    pallas_call x1, Pallas kernels, make_values(): pl.pallas_call(values_kernel, out_shape=pltpu.HBM((blocks, span + EXTRA,...  6.19 us
  transfers between devices with their start and end apart: 6, of which 3 were waited for; matrix products, arithmetic and copies ran while one was open for 0% of the time, Pallas kernels for 9%

profile of v5, /device:TPU:32, one launch (start us, length us, event | category | flops | bytes accessed | tf_op | source)
XLA Modules:
  0.0 202.9 jit_solution(14902656945231195516)
XLA Ops:
  0.6 0.7 dynamic-slice_bitcast_fusion
  1.4 29.2 %all_to_all.25.pieces_ref = bf16[16,2,16,128]{3,2,1,0:T(8,128)(2,1)S(1)} all-to-all(bf16[16,2,16,128]{3,2,1,0:T(8,128)(2,1)S(1)} %broadcast_in_dim.2), channel_id=1, replica_groups=mesh['y'=4,'x'=4,'z'=16,'c'=2] {'z'}, dimensions={0} | all-to-all | bytes 262144 | tf_op jit(solution)/shard_map/all_to_all | solution.py:25
  30.6 1.1 spread.1
  31.7 7.0 %all-to-all-start.1 = ((bf16[16,15,16,128]{3,2,1,0:T(8,128)(2,1)}), bf16[16,15,16,128]{3,2,1,0:T(8,128)(2,1)S(1)}, u32[]{:S(2)}, u32[]{:S(2)}) async-start(bf16[16,15,16,128]{3,2,1,0:T(8,128)(2,1)} %get-tuple-element.16), calls=%async_computation.1 | async-start | bytes 1966080 | tf_op jit(solution)/shard_map/all_to_all | solution.py:462
  38.7 4.6 %norm_halves.1 = (bf16[4,96,2048]{2,1,0:T(8,128)(2,1)}, bf16[4,104,2048]{2,1,0:T(8,128)(2,1)}) custom-call(bf16[8,96,2048]{2,1,0:T(8,128)(2,1)} %tokens_ref.1, f32[1,2048]{1,0:T(1,128)} %bitcast.20, bf16[64,512]{1,0:T(8,128)(2,1)} %shard_ref.2, bf16[64,512]{1,0:T(8,128)(2,1)} %shard_ref.3), custom_call_target="tpu_custom_call" | custom-call | tf_op jit(solution)/shard_map/norm_halves/pallas_call | solution.py:64
  43.4 1.9 collective-permute-start
  45.3 7.3 %all-to-all-done.1 = bf16[16,15,16,128]{3,2,1,0:T(8,128)(2,1)S(1)} async-done(((bf16[16,15,16,128]{3,2,1,0:T(8,128)(2,1)}), bf16[16,15,16,128]{3,2,1,0:T(8,128)(2,1)S(1)}, u32[]{:S(2)}, u32[]{:S(2)}) %all-to-all-start.1) | async-done | bytes 983072 | tf_op jit(solution)/shard_map/all_to_all | solution.py:462
  52.6 1.9 collective-permute-start.1
  54.5 23.3 %all-gather = bf16[240,16,128]{2,1,0:T(8,128)(2,1)S(1)} all-gather(bf16[15,16,128]{2,1,0:T(8,128)(2,1)S(1)} %get-tuple-element.17), channel_id=2, replica_groups=mesh['y'=4,'x'=4,'z'=16,'c'=2] {'y','x'}, dimensions={0}, use_global_device_ids=true | all-gather | bytes 1044480 | tf_op jit(solution)/shard_map/all_gather | solution.py:471
  77.8 1.9 collective-permute-start.2
  79.7 3.4 %arrange_kept.1 = (bf16[2,384,1024]{2,1,0:T(8,128)(2,1)S(1)}, bf16[4,8,512]{2,1,0:T(8,128)(2,1)S(1)}) custom-call(bf16[4,96,2048]{2,1,0:T(8,128)(2,1)} %get-tuple-element.11.kept_hbm, bf16[8,1024]{1,0:T(8,128)(2,1)S(1)} %copy-done.2, f32[1,128]{1,0:T(1,128)S(1)} %bitcast.16), custom_call_target="tpu_custom_call" | custom-call | tf_op jit(solution)/shard_map/arrange_kept/pallas_call | solution.py:207
  83.1 2.0 arrange_came.1
  85.1 1.0 partial.2.begun_ref
  86.1 1.0 partial.3.begun_ref
  87.2 2.2 %make_keys.1.key_ref = bf16[16,192,128]{2,1,0:T(8,128)(2,1)} custom-call(bf16[2,384,1024]{2,1,0:T(8,128)(2,1)S(1)} %get-tuple-element.12.kept_ref, bf16[2,384,1024]{2,1,0:T(8,128)(2,1)S(1)} %get-tuple-element.14.came_ref, bf16[2,64,512]{2,1,0:T(8,128)(2,1)S(1)} %get-tuple-element.15.shards_ref, bf16[4,4,240,128]{3,2,1,0:T(8,128)(2,1)S(1)} %collective-permute-done.1.rows_ref, ...), custom_call_target="tpu_custom_call" | custom-call | tf_op jit(solution)/shard_map/make_keys/pallas_call | solution.py:295
  89.3 6.2 %make_values.1 = bf16[16,200,128]{2,1,0:T(8,128)(2,1)} custom-call(bf16[2,384,1024]{2,1,0:T(8,128)(2,1)S(1)} %get-tuple-element.12.kept_ref, bf16[2,384,1024]{2,1,0:T(8,128)(2,1)S(1)} %get-tuple-element.14.came_ref, bf16[2,64,512]{2,1,0:T(8,128)(2,1)S(1)} %get-tuple-element.15.shards_ref, bf16[4,4,240,128]{3,2,1,0:T(8,128)(2,1)S(1)} %collective-permute-done.2.rows_ref, ...), custom_call_target="tpu_custom_call" | custom-call | tf_op jit(solution)/shard_map/make_values/pallas_call | solution.py:381
  95.5 48.1 %all_to_all.26.rows_ref = bf16[16,200,128]{2,1,0:T(8,128)(2,1)S(1)} all-to-all(bf16[16,200,128]{2,1,0:T(8,128)(2,1)} %make_values.1), channel_id=1, replica_groups=mesh['y'=4,'x'=4,'z'=16,'c'=2] {'z'}, dimensions={0} | all-to-all | bytes 1638400 | tf_op jit(solution)/shard_map/all_to_all | solution.py:475
  143.6 6.7 %all-to-all-start.2 = ((bf16[16,192,128]{2,1,0:T(8,128)(2,1)}), bf16[16,192,128]{2,1,0:T(8,128)(2,1)S(1)}, u32[]{:S(2)}, u32[]{:S(2)}) async-start(bf16[16,192,128]{2,1,0:T(8,128)(2,1)} %make_keys.1.key_ref), calls=%async_computation.2 | async-start | bytes 1572864 | tf_op jit(solution)/shard_map/all_to_all | solution.py:470
  150.4 0.6 join_first.1
  151.0 39.2 %all-to-all-done.2.rows_ref = bf16[16,192,128]{2,1,0:T(8,128)(2,1)S(1)} async-done(((bf16[16,192,128]{2,1,0:T(8,128)(2,1)}), bf16[16,192,128]{2,1,0:T(8,128)(2,1)S(1)}, u32[]{:S(2)}, u32[]{:S(2)}) %all-to-all-start.2) | async-done | bytes 786464 | tf_op jit(solution)/shard_map/all_to_all | solution.py:470
  190.2 4.5 %all-to-all-start.4 = ((f32[16,4,128]{2,1,0:T(4,128)}), f32[16,4,128]{2,1,0:T(4,128)S(1)}, u32[]{:S(2)}, u32[]{:S(2)}) async-start(f32[16,4,128]{2,1,0:T(4,128)} %join_first.1), calls=%async_computation.4 | async-start | bytes 65536 | tf_op jit(solution)/shard_map/all_to_all | solution.py:478
  194.7 3.3 %store.1 = bf16[16,192,128]{2,1,0:T(8,128)(2,1)} custom-call(bf16[16,192,128]{2,1,0:T(8,128)(2,1)} %copy-done.6), custom_call_target="tpu_custom_call" | custom-call | tf_op jit(solution)/shard_map/store/pallas_call | solution.py:397
  197.9 1.0 slice.4
  198.9 3.4 %all-to-all-done.4.rows_ref = f32[16,4,128]{2,1,0:T(4,128)S(1)} async-done(((f32[16,4,128]{2,1,0:T(4,128)}), f32[16,4,128]{2,1,0:T(4,128)S(1)}, u32[]{:S(2)}, u32[]{:S(2)}) %all-to-all-start.4) | async-done | bytes 32800 | tf_op jit(solution)/shard_map/all_to_all | solution.py:478
  (20 shorter events, 0.7 us)
Async XLA Ops:
  31.7 21.0 %all-to-all-start.1 = ((bf16[16,15,16,128]{3,2,1,0:T(8,128)(2,1)}), bf16[16,15,16,128]{3,2,1,0:T(8,128)(2,1)S(1)}, u32[]{:S(2)}, u32[]{:S(2)}) async-start(bf16[16,15,16,128]{3,2,1,0:T(8,128)(2,1)} %get-tuple-element.16), calls=%async_computation.1 | async-start | bytes 1966080 | tf_op jit(solution)/shard_map/all_to_all | solution.py:462
  38.7 41.0 %copy-start.2 = (bf16[8,1024]{1,0:T(8,128)(2,1)S(1)}, bf16[8,1024]{1,0:T(8,128)(2,1)}, u32[]{:S(2)}) copy-start(bf16[8,1024]{1,0:T(8,128)(2,1)} %query_ref.1) | copy-start | bytes 49156
  38.7 41.0 %copy-start.3 = (f32[128]{0:T(128)S(1)}, f32[128]{0:T(128)}, u32[]{:S(2)}) copy-start(f32[128]{0:T(128)} %param.14) | copy-start | bytes 1540
  43.4 39.8 %collective-permute-start = (bf16[4,104,2048]{2,1,0:T(8,128)(2,1)}, bf16[4,104,2048]{2,1,0:T(8,128)(2,1)S(1)}, u32[]{:S(2)}, u32[]{:S(2)}) collective-permute-start(bf16[4,104,2048]{2,1,0:T(8,128)(2,1)} %get-tuple-element.13), channel_id=1, source_target_pairs={{0,1},{1,0},{2,3},{3,2},{4,5},{5,4},{6,7},{7,6},{8,9},{9,8},{10,11... | collective-permute-start | bytes 5111816 | tf_op jit(solution)/shard_map/ppermute | solution.py:461
  52.6 34.5 %collective-permute-start.1 = (bf16[4,4,240,128]{3,2,1,0:T(8,128)(2,1)S(1)}, bf16[4,4,240,128]{3,2,1,0:T(8,128)(2,1)S(1)}, u32[]{:S(2)}, u32[]{:S(2)}) collective-permute-start(bf16[4,4,240,128]{3,2,1,0:T(8,128)(2,1)S(1)} %bitcast.12), channel_id=1, source_target_pairs={{0,1},{1,0},{2,3},{3,2},{4,5},{5,4},{6,7},{7,6},{8,9},{9,8},{10,11... | collective-permute-start | bytes 2949128 | tf_op jit(solution)/shard_map/ppermute | solution.py:467
  77.8 11.5 %collective-permute-start.2 = (bf16[4,4,240,128]{3,2,1,0:T(8,128)(2,1)S(1)}, bf16[4,4,240,128]{3,2,1,0:T(8,128)(2,1)S(1)}, u32[]{:S(2)}, u32[]{:S(2)}) collective-permute-start(bf16[4,4,240,128]{3,2,1,0:T(8,128)(2,1)S(1)} %bitcast.14), channel_id=1, source_target_pairs={{0,1},{1,0},{2,3},{3,2},{4,5},{5,4},{6,7},{7,6},{8,9},{9,8},{10,11... | collective-permute-start | bytes 2949128 | tf_op jit(solution)/shard_map/ppermute | solution.py:472
  79.7 5.4 %copy-start = (bf16[64,512]{1,0:T(8,128)(2,1)S(1)}, bf16[64,512]{1,0:T(8,128)(2,1)}, u32[]{:S(2)}) copy-start(bf16[64,512]{1,0:T(8,128)(2,1)} %shard_ref.2) | copy-start | bytes 196612
  85.1 1.0 copy-start.1
  86.1 1.0 copy-start.4
  87.1 2.2 %copy-start.5 = (f32[8]{0:T(128)S(1)}, f32[8]{0:T(128)}, u32[]{:S(2)}) copy-start(f32[8]{0:T(128)} %bias_ref.1) | copy-start | bytes 100
  143.6 46.5 %all-to-all-start.2 = ((bf16[16,192,128]{2,1,0:T(8,128)(2,1)}), bf16[16,192,128]{2,1,0:T(8,128)(2,1)S(1)}, u32[]{:S(2)}, u32[]{:S(2)}) async-start(bf16[16,192,128]{2,1,0:T(8,128)(2,1)} %make_keys.1.key_ref), calls=%async_computation.2 | async-start | bytes 1572864 | tf_op jit(solution)/shard_map/all_to_all | solution.py:470
  190.2 4.5 %copy-start.6 = (bf16[16,192,128]{2,1,0:T(8,128)(2,1)}, bf16[16,192,128]{2,1,0:T(8,128)(2,1)S(1)}, u32[]{:S(2)}) copy-start(bf16[16,192,128]{2,1,0:T(8,128)(2,1)S(1)} %all-to-all-done.2.rows_ref) | copy-start | bytes 2359300
  190.2 12.1 %all-to-all-start.4 = ((f32[16,4,128]{2,1,0:T(4,128)}), f32[16,4,128]{2,1,0:T(4,128)S(1)}, u32[]{:S(2)}, u32[]{:S(2)}) async-start(f32[16,4,128]{2,1,0:T(4,128)} %join_first.1), calls=%async_computation.4 | async-start | bytes 65536 | tf_op jit(solution)/shard_map/all_to_all | solution.py:478

commit v6 on v5

--- a/solution.py
+++ b/solution.py
@@ -300,18 +300,11 @@
     )(*on_chip(*x), shards_other, *on_chip(other, begun), gain.reshape(1, hd))
 
 
-def values_kernel(
-    kept_ref, came_ref, shards_ref, rows_ref, begun_ref, key_ref, query_ref, bias_ref, value_ref
-):
-    core = lax.axis_index("c")
+def weigh_kernel(key_ref, query_ref, bias_ref, weight_ref, total_ref):
     seqs, heads, width = query_ref.shape
     hd = key_ref.shape[2]
     span = key_ref.shape[1]
     kv_heads = width // hd
-    per_group = heads // kv_heads
-    x = both((kept_ref, came_ref), 1 - core)
-    shard = shards_ref[1]
-
     row = lax.broadcasted_iota(jnp.int32, (heads, 1), 0)
     bias = jnp.zeros((heads, 1), F32)
     for j in range(heads):
@@ -340,6 +333,37 @@
         after += jnp.dot(part, later, preferred_element_type=F32)
     weight_high, weight_low = high_low(jnp.exp(scores + log_keep + after))
     total_high, total_low = high_low(jnp.sum(log_keep, axis=1, keepdims=True))
+    weight_ref[0], weight_ref[1] = weight_high, weight_low
+    total_ref[0] = jnp.broadcast_to(total_high.astype(F32), total_ref.shape[1:])
+    total_ref[1] = jnp.broadcast_to(total_low.astype(F32), total_ref.shape[1:])
+
+
+def weigh(keys, query, bias):
+    _, span, hd = keys.shape
+    rows = query.shape[0] * query.shape[1]
+    here = pl.BlockSpec(memory_space=pltpu.VMEM)
+    return pl.pallas_call(
+        weigh_kernel,
+        out_shape=(pltpu.VMEM((2, rows, span), BF16), pltpu.VMEM((2, rows, hd), F32)),
+        in_specs=[here, here, pl.BlockSpec(memory_space=pltpu.SMEM)],
+        compiler_params=vmem(8),
+        name="weigh",
+    )(keys, *on_chip(query), bias)
+
+
+def values_kernel(
+    kept_ref, came_ref, shards_ref, rows_ref, begun_ref, weight_ref, total_ref, value_ref
+):
+    core = lax.axis_index("c")
+    kv_heads, hd = rows_ref.shape[0], rows_ref.shape[3]
+    seqs = value_ref.shape[0] // kv_heads
+    span = weight_ref.shape[2]
+    heads = weight_ref.shape[1] // seqs
+    per_group = heads // kv_heads
+    x = both((kept_ref, came_ref), 1 - core)
+    shard = shards_ref[1]
+    weight_high, weight_low = weight_ref[0], weight_ref[1]
+    total_high, total_low = total_ref[0], total_ref[1]
 
     for g in range(0, kv_heads, 2):
         raw = begun_ref[:, g * hd : (g + 2) * hd] + jnp.dot(
@@ -362,8 +386,8 @@
                 [
                     read_high.astype(F32),
                     read_low.astype(F32),
-                    jnp.broadcast_to(total_high[at].astype(F32), read.shape),
-                    jnp.broadcast_to(total_low[at].astype(F32), read.shape),
+                    total_high[at],
+                    total_low[at],
                 ],
                 axis=0,
             ).astype(BF16)
@@ -375,16 +399,16 @@
             ).astype(BF16)
 
 
-def make_values(x, shards_other, other, begun, keys, query, bias):
-    blocks, span, hd = keys.shape
-    here = pl.BlockSpec(memory_space=pltpu.VMEM)
+def make_values(x, shards_other, other, begun, weights, totals):
+    _, _, span = weights.shape
+    kv_heads, hd = other.shape[0], other.shape[3]
+    blocks = kv_heads * x[0].shape[1] * 2 // span
     return pl.pallas_call(
         values_kernel,
         out_shape=pltpu.HBM((blocks, span + EXTRA, hd), BF16),
-        in_specs=[here] * 7 + [pl.BlockSpec(memory_space=pltpu.SMEM)],
         compiler_params=vmem(24),
         name="make_values",
-    )(*on_chip(*x), shards_other, *on_chip(other, begun), keys, *on_chip(query), bias)
+    )(*on_chip(*x), shards_other, *on_chip(other, begun, weights, totals))
 
 
 def store_kernel(rows_ref, out_ref):
@@ -471,7 +495,8 @@
     late = lax.all_gather(late, SP).reshape(ys, xs, -1, head_dim)
     late_other = trade(late)
     begun = partial_product(x, w_value, late)
-    values = make_values(x, shards_other, late_other, begun, keys, query, stick_bias)
+    weights, totals = weigh(keys, query, stick_bias)
+    values = make_values(x, shards_other, late_other, begun, weights, totals)
     got_values = lax.all_to_all(values, "z", 0, 0, tiled=True)
     stored = store(got_keys)
     joined = join_first(got_values, ys * xs)

time: 204 us -> 204 us (level)
  transfers between devices with their start and end apart: 6 -> 6, of which waited for: 3 -> 3; matrix products, arithmetic and copies ran while one was open for 0% -> 0% of each run, Pallas kernels for 9% -> 10%
where the time goes in v6:
time: 204 us; the launch traced here: 203 us
  blocking collectives  101 us (50%)
  waiting for transfers between devices  49.9 us (24%)
  Pallas kernels  26 us (13%)
  starting transfers between devices  23.9 us (12%)
    all_to_all x1, blocking collectives, shards(): got_values = lax.all_to_all(values, 'z', 0, 0, tiled=True)  48.1 us
    all_to_all x1, waiting for transfers between devices, shards(): got_keys = lax.all_to_all(keys, 'z', 0, 0, tiled=True)  39.2 us
    all_to_all x1, blocking collectives, to_all(): lax.all_to_all(jnp.broadcast_to(piece[None], (count, *piece.shape)), axis...  29.2 us
    all_gather x1, blocking collectives, shards(): late = lax.all_gather(late, SP).reshape(ys, xs, -1, head_dim)  23.3 us
    all_to_all x1, waiting for transfers between devices, shards(): early = lax.all_to_all(early, SP, 0, 0, tiled=True)  7.35 us
    all_to_all x1, starting transfers between devices, shards(): early = lax.all_to_all(early, SP, 0, 0, tiled=True)  7.03 us
    all_to_all x1, starting transfers between devices, shards(): got_keys = lax.all_to_all(keys, 'z', 0, 0, tiled=True)  6.72 us
    pallas_call x1, Pallas kernels, norm_halves(): pl.pallas_call(norm_kernel, grid=(seqs,), out_shape=(pltpu.HBM((seqs, len...  4.62 us
  transfers between devices with their start and end apart: 6, of which 3 were waited for; matrix products, arithmetic and copies ran while one was open for 0% of the time, Pallas kernels for 10%

profile of v6, /device:TPU:32, one launch (start us, length us, event | category | flops | bytes accessed | tf_op | source)
XLA Modules:
  0.0 203.1 jit_solution(4977390225992567729)
XLA Ops:
  0.6 0.7 dynamic-slice_bitcast_fusion
  1.4 29.2 %all_to_all.25.pieces_ref = bf16[16,2,16,128]{3,2,1,0:T(8,128)(2,1)S(1)} all-to-all(bf16[16,2,16,128]{3,2,1,0:T(8,128)(2,1)S(1)} %broadcast_in_dim.2), channel_id=1, replica_groups=mesh['y'=4,'x'=4,'z'=16,'c'=2] {'z'}, dimensions={0} | all-to-all | bytes 262144 | tf_op jit(solution)/shard_map/all_to_all | solution.py:25
  30.6 1.1 spread.1
  31.7 7.0 %all-to-all-start.1 = ((bf16[16,15,16,128]{3,2,1,0:T(8,128)(2,1)}), bf16[16,15,16,128]{3,2,1,0:T(8,128)(2,1)S(1)}, u32[]{:S(2)}, u32[]{:S(2)}) async-start(bf16[16,15,16,128]{3,2,1,0:T(8,128)(2,1)} %get-tuple-element.18), calls=%async_computation.1 | async-start | bytes 1966080 | tf_op jit(solution)/shard_map/all_to_all | solution.py:486
  38.7 4.6 %norm_halves.1 = (bf16[4,96,2048]{2,1,0:T(8,128)(2,1)}, bf16[4,104,2048]{2,1,0:T(8,128)(2,1)}) custom-call(bf16[8,96,2048]{2,1,0:T(8,128)(2,1)} %tokens_ref.1, f32[1,2048]{1,0:T(1,128)} %bitcast.20, bf16[64,512]{1,0:T(8,128)(2,1)} %shard_ref.2, bf16[64,512]{1,0:T(8,128)(2,1)} %shard_ref.3), custom_call_target="tpu_custom_call" | custom-call | tf_op jit(solution)/shard_map/norm_halves/pallas_call | solution.py:64
  43.4 1.9 collective-permute-start
  45.3 7.3 %all-to-all-done.1 = bf16[16,15,16,128]{3,2,1,0:T(8,128)(2,1)S(1)} async-done(((bf16[16,15,16,128]{3,2,1,0:T(8,128)(2,1)}), bf16[16,15,16,128]{3,2,1,0:T(8,128)(2,1)S(1)}, u32[]{:S(2)}, u32[]{:S(2)}) %all-to-all-start.1) | async-done | bytes 983072 | tf_op jit(solution)/shard_map/all_to_all | solution.py:486
  52.6 1.9 collective-permute-start.1
  54.5 23.3 %all-gather = bf16[240,16,128]{2,1,0:T(8,128)(2,1)S(1)} all-gather(bf16[15,16,128]{2,1,0:T(8,128)(2,1)S(1)} %get-tuple-element.19), channel_id=2, replica_groups=mesh['y'=4,'x'=4,'z'=16,'c'=2] {'y','x'}, dimensions={0}, use_global_device_ids=true | all-gather | bytes 1044480 | tf_op jit(solution)/shard_map/all_gather | solution.py:495
  77.8 1.9 collective-permute-start.2
  79.7 3.4 %arrange_kept.1 = (bf16[2,384,1024]{2,1,0:T(8,128)(2,1)S(1)}, bf16[4,8,512]{2,1,0:T(8,128)(2,1)S(1)}) custom-call(bf16[4,96,2048]{2,1,0:T(8,128)(2,1)} %get-tuple-element.13.kept_hbm, bf16[8,1024]{1,0:T(8,128)(2,1)S(1)} %copy-done.2, f32[1,128]{1,0:T(1,128)S(1)} %bitcast.16), custom_call_target="tpu_custom_call" | custom-call | tf_op jit(solution)/shard_map/arrange_kept/pallas_call | solution.py:207
  83.1 2.0 arrange_came.1
  85.1 1.0 partial.2.begun_ref
  86.1 1.0 partial.3.begun_ref
  87.1 2.2 %make_keys.1.key_ref = bf16[16,192,128]{2,1,0:T(8,128)(2,1)} custom-call(bf16[2,384,1024]{2,1,0:T(8,128)(2,1)S(1)} %get-tuple-element.14.kept_ref, bf16[2,384,1024]{2,1,0:T(8,128)(2,1)S(1)} %get-tuple-element.16.came_ref, bf16[2,64,512]{2,1,0:T(8,128)(2,1)S(1)} %get-tuple-element.17.shards_ref, bf16[4,4,240,128]{3,2,1,0:T(8,128)(2,1)S(1)} %collective-permute-done.1.rows_ref, ...), custom_call_target="tpu_custom_call" | custom-call | tf_op jit(solution)/shard_map/make_keys/pallas_call | solution.py:295
  89.3 1.9 weigh.1
  91.2 4.5 %make_values.1 = bf16[16,200,128]{2,1,0:T(8,128)(2,1)} custom-call(bf16[2,384,1024]{2,1,0:T(8,128)(2,1)S(1)} %get-tuple-element.14.kept_ref, bf16[2,384,1024]{2,1,0:T(8,128)(2,1)S(1)} %get-tuple-element.16.came_ref, bf16[2,64,512]{2,1,0:T(8,128)(2,1)S(1)} %get-tuple-element.17.shards_ref, bf16[4,4,240,128]{3,2,1,0:T(8,128)(2,1)S(1)} %collective-permute-done.2.rows_ref, ...), custom_call_target="tpu_custom_call" | custom-call | tf_op jit(solution)/shard_map/make_values/pallas_call | solution.py:406
  95.7 48.1 %all_to_all.26.rows_ref = bf16[16,200,128]{2,1,0:T(8,128)(2,1)S(1)} all-to-all(bf16[16,200,128]{2,1,0:T(8,128)(2,1)} %make_values.1), channel_id=1, replica_groups=mesh['y'=4,'x'=4,'z'=16,'c'=2] {'z'}, dimensions={0} | all-to-all | bytes 1638400 | tf_op jit(solution)/shard_map/all_to_all | solution.py:500
  143.8 6.7 %all-to-all-start.2 = ((bf16[16,192,128]{2,1,0:T(8,128)(2,1)}), bf16[16,192,128]{2,1,0:T(8,128)(2,1)S(1)}, u32[]{:S(2)}, u32[]{:S(2)}) async-start(bf16[16,192,128]{2,1,0:T(8,128)(2,1)} %make_keys.1.key_ref), calls=%async_computation.2 | async-start | bytes 1572864 | tf_op jit(solution)/shard_map/all_to_all | solution.py:494
  151.2 39.2 %all-to-all-done.2.rows_ref = bf16[16,192,128]{2,1,0:T(8,128)(2,1)S(1)} async-done(((bf16[16,192,128]{2,1,0:T(8,128)(2,1)}), bf16[16,192,128]{2,1,0:T(8,128)(2,1)S(1)}, u32[]{:S(2)}, u32[]{:S(2)}) %all-to-all-start.2) | async-done | bytes 786464 | tf_op jit(solution)/shard_map/all_to_all | solution.py:494
  190.4 4.5 %all-to-all-start.4 = ((f32[16,4,128]{2,1,0:T(4,128)}), f32[16,4,128]{2,1,0:T(4,128)S(1)}, u32[]{:S(2)}, u32[]{:S(2)}) async-start(f32[16,4,128]{2,1,0:T(4,128)} %join_first.1), calls=%async_computation.4 | async-start | bytes 65536 | tf_op jit(solution)/shard_map/all_to_all | solution.py:503
  194.9 3.3 %store.1 = bf16[16,192,128]{2,1,0:T(8,128)(2,1)} custom-call(bf16[16,192,128]{2,1,0:T(8,128)(2,1)} %copy-done.6), custom_call_target="tpu_custom_call" | custom-call | tf_op jit(solution)/shard_map/store/pallas_call | solution.py:421
  198.1 1.0 slice.4
  199.1 3.4 %all-to-all-done.4.rows_ref = f32[16,4,128]{2,1,0:T(4,128)S(1)} async-done(((f32[16,4,128]{2,1,0:T(4,128)}), f32[16,4,128]{2,1,0:T(4,128)S(1)}, u32[]{:S(2)}, u32[]{:S(2)}) %all-to-all-start.4) | async-done | bytes 32800 | tf_op jit(solution)/shard_map/all_to_all | solution.py:503
  (21 shorter events, 1.3 us)
Async XLA Ops:
  31.7 21.0 %all-to-all-start.1 = ((bf16[16,15,16,128]{3,2,1,0:T(8,128)(2,1)}), bf16[16,15,16,128]{3,2,1,0:T(8,128)(2,1)S(1)}, u32[]{:S(2)}, u32[]{:S(2)}) async-start(bf16[16,15,16,128]{3,2,1,0:T(8,128)(2,1)} %get-tuple-element.18), calls=%async_computation.1 | async-start | bytes 1966080 | tf_op jit(solution)/shard_map/all_to_all | solution.py:486
  38.7 41.0 %copy-start.2 = (bf16[8,1024]{1,0:T(8,128)(2,1)S(1)}, bf16[8,1024]{1,0:T(8,128)(2,1)}, u32[]{:S(2)}) copy-start(bf16[8,1024]{1,0:T(8,128)(2,1)} %query_ref.1) | copy-start | bytes 49156
  38.7 41.0 %copy-start.3 = (f32[128]{0:T(128)S(1)}, f32[128]{0:T(128)}, u32[]{:S(2)}) copy-start(f32[128]{0:T(128)} %param.14) | copy-start | bytes 1540
  43.4 39.8 %collective-permute-start = (bf16[4,104,2048]{2,1,0:T(8,128)(2,1)}, bf16[4,104,2048]{2,1,0:T(8,128)(2,1)S(1)}, u32[]{:S(2)}, u32[]{:S(2)}) collective-permute-start(bf16[4,104,2048]{2,1,0:T(8,128)(2,1)} %get-tuple-element.15), channel_id=1, source_target_pairs={{0,1},{1,0},{2,3},{3,2},{4,5},{5,4},{6,7},{7,6},{8,9},{9,8},{10,11... | collective-permute-start | bytes 5111816 | tf_op jit(solution)/shard_map/ppermute | solution.py:485
  52.6 34.5 %collective-permute-start.1 = (bf16[4,4,240,128]{3,2,1,0:T(8,128)(2,1)S(1)}, bf16[4,4,240,128]{3,2,1,0:T(8,128)(2,1)S(1)}, u32[]{:S(2)}, u32[]{:S(2)}) collective-permute-start(bf16[4,4,240,128]{3,2,1,0:T(8,128)(2,1)S(1)} %bitcast.12), channel_id=1, source_target_pairs={{0,1},{1,0},{2,3},{3,2},{4,5},{5,4},{6,7},{7,6},{8,9},{9,8},{10,11... | collective-permute-start | bytes 2949128 | tf_op jit(solution)/shard_map/ppermute | solution.py:491
  77.8 13.4 %collective-permute-start.2 = (bf16[4,4,240,128]{3,2,1,0:T(8,128)(2,1)S(1)}, bf16[4,4,240,128]{3,2,1,0:T(8,128)(2,1)S(1)}, u32[]{:S(2)}, u32[]{:S(2)}) collective-permute-start(bf16[4,4,240,128]{3,2,1,0:T(8,128)(2,1)S(1)} %bitcast.14), channel_id=1, source_target_pairs={{0,1},{1,0},{2,3},{3,2},{4,5},{5,4},{6,7},{7,6},{8,9},{9,8},{10,11... | collective-permute-start | bytes 2949128 | tf_op jit(solution)/shard_map/ppermute | solution.py:496
  79.7 5.4 %copy-start = (bf16[64,512]{1,0:T(8,128)(2,1)S(1)}, bf16[64,512]{1,0:T(8,128)(2,1)}, u32[]{:S(2)}) copy-start(bf16[64,512]{1,0:T(8,128)(2,1)} %shard_ref.2) | copy-start | bytes 196612
  85.1 1.0 copy-start.1
  86.1 1.0 copy-start.5
  87.1 2.2 %copy-start.4 = (f32[8]{0:T(128)S(1)}, f32[8]{0:T(128)}, u32[]{:S(2)}) copy-start(f32[8]{0:T(128)} %bias_ref.1) | copy-start | bytes 100
  143.8 46.5 %all-to-all-start.2 = ((bf16[16,192,128]{2,1,0:T(8,128)(2,1)}), bf16[16,192,128]{2,1,0:T(8,128)(2,1)S(1)}, u32[]{:S(2)}, u32[]{:S(2)}) async-start(bf16[16,192,128]{2,1,0:T(8,128)(2,1)} %make_keys.1.key_ref), calls=%async_computation.2 | async-start | bytes 1572864 | tf_op jit(solution)/shard_map/all_to_all | solution.py:494
  190.4 4.5 %copy-start.6 = (bf16[16,192,128]{2,1,0:T(8,128)(2,1)}, bf16[16,192,128]{2,1,0:T(8,128)(2,1)S(1)}, u32[]{:S(2)}) copy-start(bf16[16,192,128]{2,1,0:T(8,128)(2,1)S(1)} %all-to-all-done.2.rows_ref) | copy-start | bytes 2359300
  190.4 12.1 %all-to-all-start.4 = ((f32[16,4,128]{2,1,0:T(4,128)}), f32[16,4,128]{2,1,0:T(4,128)S(1)}, u32[]{:S(2)}, u32[]{:S(2)}) async-start(f32[16,4,128]{2,1,0:T(4,128)} %join_first.1), calls=%async_computation.4 | async-start | bytes 65536 | tf_op jit(solution)/shard_map/all_to_all | solution.py:503
